TPU v7x, 256 devices: a whole 4x4x8 slice. The times are simulated.
256 devices in a mesh: sp: 32 (over z, y), tp: 8 (over x, core).
Axes of the slice: x: 4, y: 4, z: 8, core: 2. Of those that a mesh axis runs over, the one named last changes fastest.
Arguments:
- latent: bfloat16 [8192, 2048], P('sp'), may hold values from -6 to 6
- context: bfloat16 [1024, 2048], P('sp'), may hold values from -6 to 6
- condition: bfloat16 [2048], replicated, may hold values from -6 to 6
- context_condition: bfloat16 [2048], replicated, may hold values from -6 to 6
- gain_pre: float32 [2048], replicated, may hold values from 0.1 to 1.9
- gain_post: float32 [2048], replicated, may hold values from 0.1 to 1.9
- w_shift: bfloat16 [2048, 2048], P('sp', 'tp'), may hold values from -0.125 to 0.125
- w_scale: bfloat16 [2048, 2048], P('sp', 'tp'), may hold values from -0.125 to 0.125
- w_gate: bfloat16 [2048, 2048], P('sp', 'tp'), may hold values from -0.125 to 0.125
- w_query: bfloat16 [2048, 2048], P(None, 'tp'), may hold values from -0.13258252 to 0.13258252
- w_key: bfloat16 [2048, 2048], P(None, 'tp'), may hold values from -6.629126 to 6.629126
- w_value: bfloat16 [2048, 2048], P(None, 'tp'), may hold values from -0.125 to 0.125
- w_silu: bfloat16 [2048, 2048], P(None, 'tp'), may hold values from -0.125 to 0.125
- offset_bias: float32 [32, 15, 31], P('tp'), may hold values from 1.5 to 3.5
- w_out: bfloat16 [2048, 2048], P('tp'), may hold values from -0.125 to 0.125
Outputs:
- updated: bfloat16 [8192, 2048], P(('sp', 'tp'))
All inputs are finite; a program needn't handle non-finite values.
Results may differ from a plain program's by a relative error of at most 0.01.
Values may be sent and summed in bfloat16 or wider, within the bound.
A program may use at most 64 MiB of HBM per device.

v0:
```python
import jax
import jax.numpy as jnp
import numpy as np
from jax import lax
from jax.sharding import PartitionSpec as P

GRID_W = 64
WIN_ROWS = 8
WIN_COLS = 16


EPSILON = 1e-06


def sent_to_all(x, axis):
    copies = jnp.broadcast_to(x, (lax.axis_size(axis), *x.shape))
    return lax.all_to_all(copies, axis, split_axis=0, concat_axis=0, tiled=True)


def taken_together(x, axis):
    everything = sent_to_all(x, axis)
    return jnp.sum(everything, axis=0)


def laid_out(parts, dim):
    dims = list(parts.shape[1:])
    dims[dim] *= parts.shape[0]
    return jnp.moveaxis(parts, 0, dim).reshape(dims)


def gathered_copies(x, axis, dim):
    parts = sent_to_all(x, axis)
    return laid_out(parts, dim)


def extended_2(cells, sides, width):
    for axis, dim in sides:
        count = lax.axis_size(axis)
        ends = count - 1
        head = lax.slice_in_dim(cells, 0, width, axis=dim)
        tail = lax.slice_in_dim(cells, cells.shape[dim] - width, cells.shape[dim], axis=dim)
        cells = jnp.concatenate(
            [
                lax.ppermute(tail, axis, [(i, (i + 1) % count) for i in range(ends)]),
                cells,
                lax.ppermute(head, axis, [((i + 1) % count, i) for i in range(ends)]),
            ],
            axis=dim,
        )
    return cells


def cut_along(x, dim, devices):
    dims = x.shape
    parts = x.reshape(*dims[:dim], devices, dims[dim] // devices, *dims[dim + 1 :])
    return jnp.moveaxis(parts, dim, 0)


def sum_at_owner(x, axis, dim):
    parts = cut_along(x, dim, lax.axis_size(axis))
    arrived = lax.all_to_all(parts, axis, split_axis=0, concat_axis=0, tiled=True)
    return arrived.astype(jnp.float32).sum(axis=0)


def normalize(row_block, gain_row):
    values = row_block.astype(jnp.float32)
    return (
        values * lax.rsqrt(jnp.mean(values * values, axis=-1, keepdims=True) + EPSILON) * gain_row
    )


def modulate(row_block, gain_row, shift_row, scale_row):
    return (normalize(row_block, gain_row) * (1.0 + scale_row) + shift_row).astype(jnp.bfloat16)


def product(left, right):
    return jnp.dot(left, right, preferred_element_type=jnp.float32)


def shards(
    latent,
    context,
    condition,
    context_condition,
    gain_pre,
    gain_post,
    w_shift,
    w_scale,
    w_gate,
    w_query,
    w_key,
    w_value,
    w_silu,
    offset_bias,
    w_out,
):
    sp_index = lax.axis_index("sp")
    tp_index = lax.axis_index("tp")
    in_rows, local_cols = w_shift.shape
    tokens, model_width = latent.shape
    active = jax.nn.silu(jnp.stack([condition, context_condition]).astype(jnp.float32)).astype(
        jnp.bfloat16
    )
    own_active = lax.dynamic_slice_in_dim(active, sp_index * in_rows, in_rows, 1)
    stacked = jnp.stack([w_shift, w_scale, w_gate])
    partial_value = jnp.einsum(
        "ai,mij->maj", own_active, stacked, preferred_element_type=jnp.float32
    )
    summed = taken_together(partial_value, "sp")
    modulation = gathered_copies(summed, "tp", 2)
    shifts, scales, gating = (modulation[0], modulation[1], modulation[2])
    normed = modulate(context, gain_pre, shifts[1], scales[1])
    context_kv = gathered_copies(
        jnp.concatenate([product(normed, w_key), product(normed, w_value)], axis=1).astype(
            jnp.bfloat16
        ),
        "sp",
        0,
    )
    hidden = modulate(latent, gain_pre, shifts[0], scales[0])
    queries = product(hidden, w_query).astype(jnp.bfloat16)
    keys_latent = product(hidden, w_key).astype(jnp.bfloat16)
    values_latent = product(hidden, w_value).astype(jnp.bfloat16)
    silu_gate = product(hidden, w_silu).astype(jnp.bfloat16)
    head_count = offset_bias.shape[0]
    head_width = local_cols // head_count
    grid_rows = tokens // GRID_W
    kv_grid = jnp.concatenate([keys_latent, values_latent], axis=1).reshape(
        grid_rows, GRID_W, 2 * local_cols
    )
    extended = extended_2(kv_grid, (("sp", 0),), WIN_ROWS // 2)
    blocks = GRID_W // WIN_COLS
    key_span = 2 * WIN_COLS
    block_start = np.clip(np.arange(blocks) * WIN_COLS - WIN_COLS // 2, 0, GRID_W - key_span)
    query_col = np.arange(blocks)[:, None] * WIN_COLS + np.arange(WIN_COLS)[None, :]
    key_col = block_start[:, None] + np.arange(key_span)[None, :]
    window_start = np.clip(query_col - WIN_COLS // 2, 0, GRID_W - WIN_COLS)
    inside_cols = (key_col[:, None, :] >= window_start[:, :, None]) & (
        key_col[:, None, :] < window_start[:, :, None] + WIN_COLS
    )
    inside_window = np.broadcast_to(
        inside_cols[:, :, None, :], (blocks, WIN_COLS, WIN_ROWS, key_span)
    ).reshape(blocks, WIN_COLS, WIN_ROWS * key_span)[None, :, None, :, :]
    col_offset = np.clip(
        key_col[:, None, :] - query_col[:, :, None] + WIN_COLS - 1, 0, 2 * WIN_COLS - 2
    )
    col_table = (col_offset[..., None] == np.arange(2 * WIN_COLS - 1)).astype(np.float32)
    total_rows = grid_rows * lax.axis_size("sp")
    local_rows = jnp.arange(grid_rows, dtype=jnp.int32)
    global_row = sp_index * grid_rows + local_rows
    row_start = jnp.clip(global_row - WIN_ROWS // 2, 0, total_rows - WIN_ROWS)
    band_first = row_start - sp_index * grid_rows + WIN_ROWS // 2
    row_offset = (
        row_start[:, None]
        + jnp.arange(WIN_ROWS, dtype=jnp.int32)[None, :]
        - global_row[:, None]
        + WIN_ROWS
        - 1
    )
    row_table = (row_offset[..., None] == jnp.arange(2 * WIN_ROWS - 1, dtype=jnp.int32)).astype(
        jnp.float32
    )
    position = (
        band_first[:, None, None, None] + jnp.arange(WIN_ROWS, dtype=jnp.int32)[None, None, :, None]
    ) * GRID_W + jnp.asarray(key_col, jnp.int32)[None, :, None, :]
    flat_rows = extended.reshape(-1, 2 * local_cols)
    window_kv = jnp.take(flat_rows, position.reshape(-1), axis=0).reshape(
        grid_rows, blocks, WIN_ROWS * key_span, 2 * local_cols
    )
    window_keys = window_kv[..., :local_cols].reshape(
        grid_rows, blocks, WIN_ROWS * key_span, head_count, head_width
    )
    window_values = window_kv[..., local_cols:].reshape(
        grid_rows, blocks, WIN_ROWS * key_span, head_count, head_width
    )
    context_keys = context_kv[:, :local_cols].reshape(-1, head_count, head_width)
    context_values = context_kv[:, local_cols:].reshape(-1, head_count, head_width)
    query_blocks = queries.reshape(grid_rows, blocks, WIN_COLS, head_count, head_width)
    score_scale = head_width ** (-0.5)
    by_column = jnp.einsum("hae,bqwe->hbqwa", offset_bias, jnp.asarray(col_table))
    offset_terms = jnp.einsum("rva,hbqwa->rbhqvw", row_table, by_column).reshape(
        grid_rows, blocks, head_count, WIN_COLS, WIN_ROWS * key_span
    )
    window_scores = (
        jnp.einsum(
            "rbqhd,rbkhd->rbhqk", query_blocks, window_keys, preferred_element_type=jnp.float32
        )
        * score_scale
    )
    window_scores = jnp.where(inside_window, window_scores + offset_terms, -jnp.inf)
    context_scores = (
        jnp.einsum(
            "rbqhd,khd->rbhqk", query_blocks, context_keys, preferred_element_type=jnp.float32
        )
        * score_scale
    )
    maximum = jnp.maximum(jnp.max(window_scores, axis=-1), jnp.max(context_scores, axis=-1))[
        ..., None
    ]
    window_exp = jnp.exp(window_scores - maximum)
    context_exp = jnp.exp(context_scores - maximum)
    denominator = jnp.sum(window_exp, axis=-1, keepdims=True) + jnp.sum(
        context_exp, axis=-1, keepdims=True
    )
    window_weights = (window_exp / denominator).astype(jnp.bfloat16)
    context_weights = (context_exp / denominator).astype(jnp.bfloat16)
    attended = jnp.einsum(
        "rbhqk,rbkhd->rbqhd", window_weights, window_values, preferred_element_type=jnp.float32
    )
    attended = attended + jnp.einsum(
        "rbhqk,khd->rbqhd", context_weights, context_values, preferred_element_type=jnp.float32
    )
    attended = attended.reshape(tokens, local_cols)
    gated_heads = (jax.nn.silu(silu_gate.astype(jnp.float32)) * attended).astype(jnp.bfloat16)
    out_rows = tokens // lax.axis_size("tp")
    branch = sum_at_owner(product(gated_heads, w_out).astype(jnp.bfloat16), "tp", 0).astype(
        jnp.bfloat16
    )
    own_rows = lax.dynamic_slice_in_dim(latent, tp_index * out_rows, out_rows, 0)
    updated = own_rows.astype(jnp.float32) + gating[0] * normalize(branch, gain_post)
    return updated.astype(jnp.bfloat16)


def solution(mesh):
    in_specs = (
        P("sp", None),
        P("sp", None),
        P(),
        P(),
        P(),
        P(),
        P("sp", "tp"),
        P("sp", "tp"),
        P("sp", "tp"),
        P(None, "tp"),
        P(None, "tp"),
        P(None, "tp"),
        P(None, "tp"),
        P("tp", None, None),
        P("tp", None),
    )
    out_specs = P(("sp", "tp"), None)
    return jax.shard_map(shards, mesh=mesh, in_specs=in_specs, out_specs=out_specs, check_vma=False)
```

profile of v0, /device:TPU:32, one launch (start us, length us, event | category | flops | bytes accessed | tf_op | source)
XLA Modules:
  0.0 143.3 jit_solution(17600305980585460209)
XLA Ops:
  0.0 0.8 stack.25
  0.9 0.7 stack.26
  1.6 1.0 convolution_bitcast_fusion.2
  2.6 0.7 broadcast_in_dim.26
  3.3 11.4 %all-to-all-start = ((f32[32,3,2,256]{3,2,1,0:T(2,128)}), f32[32,3,2,256]{3,2,1,0:T(2,128)S(1)}, u32[]{:S(2)}, u32[]{:S(2)}) async-start(f32[32,3,2,256]{3,2,1,0:T(2,128)} %broadcast_in_dim.26), calls=%async_computation | async-start | bytes 393216 | tf_op jit(solution)/shard_map/all_to_all | solution.py:17
  14.7 1.5 %fusion.2 = f32[256]{0:T(256)S(1)} fusion(bf16[256,2048]{1,0:T(8,128)(2,1)} %param.18), kind=kLoop, calls=%fused_computation.11 | loop fusion | flops 1572608 | bytes 1049600 | tf_op jit(solution)/shard_map/reduce_sum | solution.py:68
  16.3 0.1 add_multiply_fusion
  16.3 0.8 broadcast_add_fusion
  17.1 0.1 add.268
  17.2 0.1 add.256
  17.3 0.1 add.257
  17.4 0.1 add.260
  17.5 0.1 subtract_add_fusion
  17.6 0.1 fusion.22
  17.7 3.5 %convolution_bitcast_fusion = f32[4,4,4,16,8,32]{5,4,0,3,1,2:T(8,128)} fusion(bf16[4,16,32,31,1]{3,2,1,0,4:T(8,128)(2,1)S(1)} %copy-done.9, f32[4,15,31,1,1]{2,0,1,4,3:T(4,128)S(1)} %bitcast.100, s32[4,8]{1,0:T(4,128)S(1)} %subtract_add_fusion), kind=kOutput, calls=%fused_computation.10 | convolution fusion | flops 15483360 | bytes 1183120 | tf_op jit(solution)/shard_map/rva,hbqwa->rbhqvw/dot_general | solution.py:181
  21.2 4.4 %all-to-all-done = f32[32,3,2,256]{3,2,1,0:T(2,128)S(1)} async-done(((f32[32,3,2,256]{3,2,1,0:T(2,128)}), f32[32,3,2,256]{3,2,1,0:T(2,128)S(1)}, u32[]{:S(2)}, u32[]{:S(2)}) %all-to-all-start) | async-done | bytes 196640 | tf_op jit(solution)/shard_map/all_to_all | solution.py:17
  25.6 0.1 reduce_sum.66
  25.6 0.6 broadcast_in_dim.31
  26.3 4.3 %all-to-all-start.1 = ((f32[8,3,2,256]{3,2,1,0:T(2,128)}), f32[8,3,2,256]{3,2,1,0:T(2,128)S(1)}, u32[]{:S(2)}, u32[]{:S(2)}) async-start(f32[8,3,2,256]{3,2,1,0:T(2,128)} %broadcast_in_dim.31), calls=%async_computation.1 | async-start | bytes 98304 | tf_op jit(solution)/shard_map/all_to_all | solution.py:17
  30.6 0.0 copy-start.11
  30.6 3.5 %reshape.255 = f32[4,4,4,16,256]{4,0,3,1,2:T(4,128)S(1)} reshape(f32[4,4,4,16,8,32]{5,4,0,3,1,2:T(8,128)} %convolution_bitcast_fusion) | data formatting | bytes 2097152 | tf_op jit(solution)/shard_map/reshape | solution.py:181
  34.1 2.0 %all-to-all-done.1 = f32[8,3,2,256]{3,2,1,0:T(2,128)S(1)} async-done(((f32[8,3,2,256]{3,2,1,0:T(2,128)}), f32[8,3,2,256]{3,2,1,0:T(2,128)S(1)}, u32[]{:S(2)}, u32[]{:S(2)}) %all-to-all-start.1) | async-done | bytes 49184 | tf_op jit(solution)/shard_map/all_to_all | solution.py:17
  36.2 1.6 %convolution_convert_fusion.6 = bf16[32,256]{1,0:T(8,128)(2,1)S(1)} fusion(bf16[2048,256]{1,0:T(8,128)(2,1)} %param.28, bf16[32,2048]{1,0:T(8,128)(2,1)S(1)} %copy-done.7, f32[2048]{0:T(1024)S(1)} %bitcast.94, f32[2048]{0:T(1024)S(1)} %bitcast.96, f32[2048]{0:T(1024)S(1)} %copy-done.11, f32[32]{0:T(128)S(1)} %add_rsqrt_fusion.2), kind=kOutput, calls=%fused_computation.32 | convolution fusion | flops 33955840 | bytes 1220736 | tf_op jit(solution)/shard_map/dot_general | solution.py:77
  37.7 1.6 %convolution_convert_fusion.5 = bf16[32,256]{1,0:T(8,128)(2,1)S(1)} fusion(bf16[2048,256]{1,0:T(8,128)(2,1)} %param.29, bf16[32,2048]{1,0:T(8,128)(2,1)S(1)} %copy-done.7, f32[2048]{0:T(1024)S(1)} %bitcast.95, f32[2048]{0:T(1024)S(1)} %bitcast.97, f32[2048]{0:T(1024)S(1)} %copy-done.11, f32[32]{0:T(128)S(1)} %add_rsqrt_fusion.2), kind=kOutput, calls=%fused_computation.31 | convolution fusion | flops 33955840 | bytes 1220736 | tf_op jit(solution)/shard_map/dot_general | solution.py:77
  39.3 1.1 broadcast_in_dim.59
  40.4 5.5 %all-to-all-start.2 = ((bf16[32,32,512]{2,1,0:T(8,128)(2,1)}), bf16[32,32,512]{2,1,0:T(8,128)(2,1)}, u32[]{:S(2)}, u32[]{:S(2)}) async-start(bf16[32,32,512]{2,1,0:T(8,128)(2,1)} %broadcast_in_dim.59), calls=%async_computation.2 | async-start | bytes 2097152 | tf_op jit(solution)/shard_map/all_to_all | solution.py:17
  45.8 0.0 copy-start.5
  45.9 0.0 copy-start.8
  45.9 2.5 %convolution_convert_fusion.2 = bf16[256,256]{0,1:T(8,128)(2,1)S(1)} fusion(bf16[2048,256]{1,0:T(8,128)(2,1)} %param.29, bf16[256,2048]{1,0:T(8,128)(2,1)} %param.18, f32[2048]{0:T(1024)S(1)} %bitcast.101, f32[2048]{0:T(1024)S(1)} %bitcast.105, f32[2048]{0:T(1024)S(1)} %copy-done.11, f32[256]{0:T(256)S(1)} %add_rsqrt_fusion), kind=kOutput, calls=%fused_computation.27 | convolution fusion | flops 271646720 | bytes 2253824 | tf_op jit(solution)/shard_map/dot_general | solution.py:77
  48.3 0.8 convolution_convert_fusion.3
  49.2 0.1 copy.81
  49.3 3.4 %collective-permute-start = (bf16[4,64,512]{2,1,0:T(8,128)(2,1)S(1)}, bf16[4,64,512]{2,1,0:T(8,128)(2,1)S(1)}, u32[]{:S(2)}, u32[]{:S(2)}) collective-permute-start(bf16[4,64,512]{2,1,0:T(8,128)(2,1)S(1)} %bitcast.89), channel_id=1, source_target_pairs={{0,8},{8,16},{16,24},{24,32},{32,40},{40,48},{48,56},{56,64},{64,7... | collective-permute-start | bytes 786440 | tf_op jit(solution)/shard_map/ppermute | solution.py:44
  52.7 4.8 %collective-permute-start.1 = (bf16[4,64,512]{2,1,0:T(8,128)(2,1)S(1)}, bf16[4,64,512]{2,1,0:T(8,128)(2,1)}, u32[]{:S(2)}, u32[]{:S(2)}) collective-permute-start(bf16[4,64,512]{2,1,0:T(8,128)(2,1)S(1)} %bitcast.90), channel_id=1, source_target_pairs={{8,0},{16,8},{24,16},{32,24},{40,32},{48,40},{56,48},{64,56},{72,6... | collective-permute-start | bytes 786440 | tf_op jit(solution)/shard_map/ppermute | solution.py:46
  57.5 2.1 %convolution_convert_fusion.1 = bf16[256,256]{1,0:T(8,128)(2,1)S(1)} fusion(bf16[2048,256]{1,0:T(8,128)(2,1)} %param.27, bf16[256,2048]{1,0:T(8,128)(2,1)} %param.18, f32[2048]{0:T(1024)S(1)} %bitcast.103, f32[2048]{0:T(1024)S(1)} %bitcast.107, f32[2048]{0:T(1024)S(1)} %copy-done.11, f32[256]{0:T(256)S(1)} %add_rsqrt_fusion), kind=kOutput, calls=%fused_computation.26 | convolution fusion | flops 271646720 | bytes 2253824 | tf_op jit(solution)/shard_map/dot_general | solution.py:77
  59.6 0.2 reshape.232
  59.7 17.3 %collective-permute-done = bf16[4,64,512]{2,1,0:T(8,128)(2,1)S(1)} collective-permute-done((bf16[4,64,512]{2,1,0:T(8,128)(2,1)S(1)}, bf16[4,64,512]{2,1,0:T(8,128)(2,1)S(1)}, u32[]{:S(2)}, u32[]{:S(2)}) %collective-permute-start) | collective-permute-done | bytes 262176 | tf_op jit(solution)/shard_map/ppermute | solution.py:44
  77.0 0.7 copy-done.10
  77.7 1.1 pad_maximum_fusion
  78.9 17.3 %gather_fusion = bf16[4096,512]{1,0:T(8,128)(2,1)} fusion(bf16[768,512]{1,0:T(8,128)(2,1)S(1)} %bitcast.83, s32[4096]{0:T(1024)S(1)} %broadcast_clamp_fusion), kind=kCustom, calls=%fused_computation | custom fusion | bytes 8404992 | tf_op jit(solution)/shard_map/jit(_take)/gather | solution.py:167
  96.1 7.3 %copy.82 = bf16[4,4,256,512]{2,3,1,0:T(8,128)(2,1)} copy(bf16[4,4,256,512]{3,2,1,0:T(8,128)(2,1)} %bitcast.84) | data formatting | bytes 8388608 | tf_op jit(solution)/shard_map/jit(_take)/gather | solution.py:167
  103.4 2.6 %broadcast_select_fusion = bf16[4,4,256,512]{2,3,1,0:T(8,128)(2,1)S(1)} fusion(bf16[4,4,256,512]{2,3,1,0:T(8,128)(2,1)} %copy.82, pred[4,4,256]{2,1,0:T(4,128)(4,1)S(1)} %fusion.45), kind=kLoop, calls=%fused_computation.5 | loop fusion | flops 2097152 | bytes 8392704 | tf_op jit(solution)/shard_map/jit(_take)/select_n | solution.py:167
  106.0 0.0 copy-start.12
  106.0 1.7 %fusion.62 = (bf16[4,4,256,256]{2,3,1,0:T(8,128)(2,1)}, bf16[4,4,256,256]{2,3,1,0:T(8,128)(2,1)S(1)}) fusion(bf16[4,4,256,512]{2,3,1,0:T(8,128)(2,1)S(1)} %broadcast_select_fusion), kind=kLoop, calls=%fused_computation.96 | loop fusion | bytes 8388608 | tf_op jit(solution)/shard_map/slice | solution.py:173
  107.7 1.5 %fusion.65 = (f32[4,4,4,16]{3,2,1,0:T(4,128)S(1)}, f32[4,4,4,16,256]{4,3,2,1,0:T(8,128)}) fusion(f32[4,4,4,16,256]{4,0,3,1,2:T(4,128)S(1)} %reshape.255, bf16[4,4,256,4,64]{2,4,3,1,0:T(8,128)(2,1)S(1)} %bitcast.85, bf16[4,4,16,4,64]{4,3,2,1,0:T(4,128)(2,1)S(1)} %reshape.232, pred[4,16,256]{2,1,0:T(8,128)(4,1)S(1)} %copy-done.12), kind=kOutput, calls=%fused_computation.99 | convolution fusion | flops 34601984 | bytes 4345856 | tf_op jit(solution)/shard_map/rbqhd,rbkhd->rbhqk/dot_general | solution.py:185
  109.1 2.0 %fusion.63 = (bf16[1024,256]{1,0:T(8,128)(2,1)S(1)}, bf16[1024,256]{1,0:T(8,128)(2,1)}) fusion(bf16[1024,512]{1,0:T(8,128)(2,1)} %bitcast.25), kind=kLoop, calls=%fused_computation.97 | loop fusion | bytes 2097152 | tf_op jit(solution)/shard_map/slice | solution.py:176
  111.2 0.2 copy.86
  111.4 0.8 bitcast_reduce_fusion
  112.3 0.4 copy-done.2
  112.6 0.4 fusion.19
  113.1 1.0 fusion.1
  114.0 0.1 copy-done.1
  114.2 0.3 copy-done.3
  114.5 0.2 copy.91
  114.7 3.0 %fusion.14 = f32[4,4,16,4,64]{4,2,3,1,0:T(8,128)S(1)} fusion(bf16[1024,4,64,1,1]{0,2,1,4,3:T(8,128)(2,1)S(1)} %bitcast.92, f32[4,1024,4,4,16]{1,4,3,2,0:T(8,128)} %copy-done.1, f32[4,4,4,16]{3,1,0,2:T(4,128)S(1)} %copy.92, f32[4,4,4,16]{3,1,0,2:T(4,128)S(1)} %copy.89), kind=kOutput, calls=%fused_computation.23 | convolution fusion | flops 138412032 | bytes 4988928 | tf_op jit(solution)/shard_map/rbhqk,khd->rbqhd/dot_general | solution.py:210
  117.7 0.0 copy-start.6
  117.7 0.8 fusion.17
  118.5 0.2 copy.94
  118.7 0.3 reshape.238
  119.1 3.6 %convolution_convert_fusion = bf16[256,2048]{1,0:T(8,128)(2,1)} fusion(bf16[256,2048]{1,0:T(8,128)(2,1)S(1)} %copy-done, f32[256,256]{1,0:T(8,128)S(1)} %reshape.238, bf16[2048,256]{1,0:T(8,128)(2,1)} %param.30, bf16[256,2048]{1,0:T(8,128)(2,1)S(1)} %copy-done.6, f32[2048]{0:T(1024)S(1)} %bitcast.104, f32[2048]{0:T(1024)S(1)} %bitcast.108, ...), kind=kOutput, calls=%fused_computation.9 | convolution fusion | flops 541065216 | bytes 4482048 | tf_op jit(solution)/shard_map/dot_general | solution.py:77
  122.6 3.7 %all-to-all-start.3 = ((bf16[8,32,2048]{2,1,0:T(8,128)(2,1)}), bf16[8,32,2048]{2,1,0:T(8,128)(2,1)S(1)}, u32[]{:S(2)}, u32[]{:S(2)}) async-start(bf16[8,32,2048]{2,1,0:T(8,128)(2,1)} %bitcast.88), calls=%async_computation.3 | async-start | bytes 2097152 | tf_op jit(solution)/shard_map/all_to_all | solution.py:61
  126.3 15.9 %all-to-all-done.3 = bf16[8,32,2048]{2,1,0:T(8,128)(2,1)S(1)} async-done(((bf16[8,32,2048]{2,1,0:T(8,128)(2,1)}), bf16[8,32,2048]{2,1,0:T(8,128)(2,1)S(1)}, u32[]{:S(2)}, u32[]{:S(2)}) %all-to-all-start.3) | async-done | bytes 1048608 | tf_op jit(solution)/shard_map/all_to_all | solution.py:61
  142.2 0.1 reduce_sum.71
  142.3 0.1 fusion.27
  142.5 0.8 fusion.31
  (42 shorter events, 0.3 us)
Async XLA Ops:
  0.0 119.1 %copy-start = (bf16[256,2048]{1,0:T(8,128)(2,1)S(1)}, bf16[256,2048]{1,0:T(8,128)(2,1)}, u32[]{:S(2)}) copy-start(bf16[256,2048]{1,0:T(8,128)(2,1)} %param.32) | copy-start | bytes 3145732
  0.0 17.4 %copy-start.15 = (s32[4,32]{1,0:T(4,128)S(1)}, s32[4,32]{1,0:T(4,128)}, u32[]{:S(2)}) copy-start(s32[4,32]{1,0:T(4,128)} %constant.77.clone) | copy-start | bytes 1540
  0.0 17.7 %copy-start.9 = (bf16[4,16,32,31,1]{3,2,1,0,4:T(8,128)(2,1)S(1)}, bf16[4,16,32,31,1]{3,2,1,0,4:T(8,128)(2,1)}, u32[]{:S(2)}) copy-start(bf16[4,16,32,31,1]{3,2,1,0,4:T(8,128)(2,1)} %constant.148) | copy-start | bytes 380932
  0.0 17.6 %copy-start.7 = (bf16[32,2048]{1,0:T(8,128)(2,1)S(1)}, bf16[32,2048]{1,0:T(8,128)(2,1)}, u32[]{:S(2)}) copy-start(bf16[32,2048]{1,0:T(8,128)(2,1)} %param.19) | copy-start | bytes 393220
  0.0 17.7 %copy-start.13 = (f32[4,15,31]{2,0,1:T(4,128)S(1)}, f32[4,15,31]{2,0,1:T(4,128)}, u32[]{:S(2)}) copy-start(f32[4,15,31]{2,0,1:T(4,128)} %param.31) | copy-start | bytes 22324
  3.3 22.2 %all-to-all-start = ((f32[32,3,2,256]{3,2,1,0:T(2,128)}), f32[32,3,2,256]{3,2,1,0:T(2,128)S(1)}, u32[]{:S(2)}, u32[]{:S(2)}) async-start(f32[32,3,2,256]{3,2,1,0:T(2,128)} %broadcast_in_dim.26), calls=%async_computation | async-start | bytes 393216 | tf_op jit(solution)/shard_map/all_to_all | solution.py:17
  26.3 9.8 %all-to-all-start.1 = ((f32[8,3,2,256]{3,2,1,0:T(2,128)}), f32[8,3,2,256]{3,2,1,0:T(2,128)S(1)}, u32[]{:S(2)}, u32[]{:S(2)}) async-start(f32[8,3,2,256]{3,2,1,0:T(2,128)} %broadcast_in_dim.31), calls=%async_computation.1 | async-start | bytes 98304 | tf_op jit(solution)/shard_map/all_to_all | solution.py:17
  30.6 5.6 %copy-start.11 = (f32[2048]{0:T(1024)S(1)}, f32[2048]{0:T(1024)}, u32[]{:S(2)}) copy-start(f32[2048]{0:T(1024)} %param.22) | copy-start | bytes 24580
  40.4 68.8 %all-to-all-start.2 = ((bf16[32,32,512]{2,1,0:T(8,128)(2,1)}), bf16[32,32,512]{2,1,0:T(8,128)(2,1)}, u32[]{:S(2)}, u32[]{:S(2)}) async-start(bf16[32,32,512]{2,1,0:T(8,128)(2,1)} %broadcast_in_dim.59), calls=%async_computation.2 | async-start | bytes 2097152 | tf_op jit(solution)/shard_map/all_to_all | solution.py:17
  45.8 2.5 %copy-start.5 = (bf16[256,2048]{1,0:T(8,128)(2,1)S(1)}, bf16[256,2048]{1,0:T(8,128)(2,1)}, u32[]{:S(2)}) copy-start(bf16[256,2048]{1,0:T(8,128)(2,1)} %param.18) | copy-start | bytes 3145732
  45.9 2.5 %copy-start.8 = (bf16[2048,256]{1,0:T(8,128)(2,1)S(1)}, bf16[2048,256]{1,0:T(8,128)(2,1)}, u32[]{:S(2)}) copy-start(bf16[2048,256]{1,0:T(8,128)(2,1)} %param.28) | copy-start | bytes 3145732
  49.3 27.7 %collective-permute-start = (bf16[4,64,512]{2,1,0:T(8,128)(2,1)S(1)}, bf16[4,64,512]{2,1,0:T(8,128)(2,1)S(1)}, u32[]{:S(2)}, u32[]{:S(2)}) collective-permute-start(bf16[4,64,512]{2,1,0:T(8,128)(2,1)S(1)} %bitcast.89), channel_id=1, source_target_pairs={{0,8},{8,16},{16,24},{24,32},{32,40},{40,48},{48,56},{56,64},{64,7... | collective-permute-start | bytes 786440 | tf_op jit(solution)/shard_map/ppermute | solution.py:44
  52.7 25.0 %collective-permute-start.1 = (bf16[4,64,512]{2,1,0:T(8,128)(2,1)S(1)}, bf16[4,64,512]{2,1,0:T(8,128)(2,1)}, u32[]{:S(2)}, u32[]{:S(2)}) collective-permute-start(bf16[4,64,512]{2,1,0:T(8,128)(2,1)S(1)} %bitcast.90), channel_id=1, source_target_pairs={{8,0},{16,8},{24,16},{32,24},{40,32},{48,40},{56,48},{64,56},{72,6... | collective-permute-start | bytes 786440 | tf_op jit(solution)/shard_map/ppermute | solution.py:46
  77.0 0.7 copy-start.10
  106.0 1.7 %copy-start.12 = (pred[4,16,256]{2,1,0:T(8,128)(4,1)S(1)}, pred[4,16,256]{2,1,0:T(8,128)(4,1)}, u32[]{:S(2)}) copy-start(pred[4,16,256]{2,1,0:T(8,128)(4,1)} %constant.81) | copy-start | bytes 49156
  111.4 1.2 copy-start.2
  112.2 1.9 %copy-start.1 = (f32[4,1024,4,4,16]{1,4,3,2,0:T(8,128)}, f32[4,1024,4,4,16]{1,4,3,2,0:T(8,128)S(1)}, u32[]{:S(2)}) copy-start(f32[4,1024,4,4,16]{1,4,3,2,0:T(8,128)S(1)} %get-tuple-element.17) | copy-start | bytes 12582916
  113.1 1.4 %copy-start.3 = (bf16[1024,256]{1,0:T(8,128)(2,1)S(1)}, bf16[1024,256]{1,0:T(8,128)(2,1)}, u32[]{:S(2)}) copy-start(bf16[1024,256]{1,0:T(8,128)(2,1)} %get-tuple-element.8) | copy-start | bytes 1572868
  114.7 3.0 %copy-start.4 = (bf16[4,4,256,256]{2,3,1,0:T(8,128)(2,1)S(1)}, bf16[4,4,256,256]{2,3,1,0:T(8,128)(2,1)}, u32[]{:S(2)}) copy-start(bf16[4,4,256,256]{2,3,1,0:T(8,128)(2,1)} %get-tuple-element.5) | copy-start | bytes 6291460
  117.7 1.3 copy-start.6
  122.6 19.9 %copy-start.14 = (f32[2048]{0:T(1024)S(1)}, f32[2048]{0:T(1024)}, u32[]{:S(2)}) copy-start(f32[2048]{0:T(1024)} %param.23) | copy-start | bytes 24580
  122.6 19.6 %all-to-all-start.3 = ((bf16[8,32,2048]{2,1,0:T(8,128)(2,1)}), bf16[8,32,2048]{2,1,0:T(8,128)(2,1)S(1)}, u32[]{:S(2)}, u32[]{:S(2)}) async-start(bf16[8,32,2048]{2,1,0:T(8,128)(2,1)} %bitcast.88), calls=%async_computation.3 | async-start | bytes 2097152 | tf_op jit(solution)/shard_map/all_to_all | solution.py:61
where the time goes:
time: 144 us; the launch traced here: 143 us
  waiting for transfers between devices  39.6 us (28%)
  local copies, waits for them, and re-layouts  38.9 us (27%)
  starting transfers between devices  32.9 us (23%)
  matrix products  22.5 us (16%)
  other arithmetic  9.02 us (6%)
    gather x2, local copies, waits for them, and re-layouts, shards(): jnp.take(flat_rows, position.reshape(-1), axis=0)  24.5 us
    all_to_all x3, starting transfers between devices, sent_to_all(): return lax.all_to_all(copies, axis, split_axis=0, concat_axis=0, tiled=True)  21.1 us
    ppermute x1, waiting for transfers between devices, extended_2(): lax.ppermute(tail, axis, [(i, (i + 1) % count) for i in range(ends)])  17.3 us
    all_to_all x1, waiting for transfers between devices, sum_at_owner(): lax.all_to_all(parts, axis, split_axis=0, concat_axis=0, tiled=True)  15.9 us
    dot_general x6, matrix products, product(): return jnp.dot(left, right, preferred_element_type=jnp.float32)  12 us
    all_to_all x3, waiting for transfers between devices, sent_to_all(): return lax.all_to_all(copies, axis, split_axis=0, concat_axis=0, tiled=True)  6.41 us
    ppermute x1, starting transfers between devices, extended_2(): lax.ppermute(head, axis, [((i + 1) % count, i) for i in range(ends)])  4.76 us
    all_to_all x1, starting transfers between devices, sum_at_owner(): lax.all_to_all(parts, axis, split_axis=0, concat_axis=0, tiled=True)  3.69 us
  transfers between devices with their start and end apart: 6, of which 4 were waited for; matrix products, arithmetic and copies ran while one was open for 33% of the time, Pallas kernels for 0%

commit v1 on v0

v1 whole, which is shorter than its diff:
```python
import functools

import jax
import jax.numpy as jnp
from jax import lax
from jax.experimental import pallas as pl
from jax.experimental.pallas import tpu as pltpu
from jax.sharding import PartitionSpec as P

GRID_W = 64
WIN_ROWS = 8
WIN_COLS = 16
EPSILON = 1e-06
NZ, NY, NX, NC = 8, 4, 4, 2
NTP = NX * NC
D = 2048
HD = 64
TOK = 256
CTXL = 32
CTX = 1024
OUTR = TOK // NTP
LAST_START = NZ * NY * TOK // GRID_W - WIN_ROWS
SPECIAL = (0, 1, 2, 6, 7)
F32 = jnp.float32
BF16 = jnp.bfloat16
NT = (((1,), (1,)), ((), ()))


def dot(a, b):
    return jnp.dot(a, b, preferred_element_type=F32)


def dot_nt(a, b):
    return lax.dot_general(a, b, NT, preferred_element_type=F32)


def remote(src, dst, ssem, rsem, sp, tp):
    return pltpu.make_async_remote_copy(
        src_ref=src,
        dst_ref=dst,
        send_sem=ssem,
        recv_sem=rsem,
        device_id=(sp, tp),
        device_id_type=pl.DeviceIdType.MESH,
    )


def half_swap(v):
    return pltpu.roll(v, 64, 1)


def kernel(
    act_ref,
    biasx_ref,
    gpre_ref,
    gpost_ref,
    lat_h,
    ctx_h,
    wsh_h,
    wsc_h,
    wga_h,
    wq_h,
    wk_h,
    wv_h,
    wg_h,
    wo_h,
    out_ref,
    wmod,
    lat,
    ctx,
    wkv,
    wqg,
    wo,
    wo2,
    zsend,
    zrecv,
    msend,
    mrecv,
    mod,
    btab,
    hid,
    hidc,
    rsl,
    rsc,
    csend,
    ctxkv,
    kvsend,
    kvext,
    qsend,
    qrecv,
    sg,
    rsend,
    rrecv,
    gated,
    grecv,
    psend,
    precv,
    lsem,
    zs,
    zr,
    ms,
    mr,
    ws,
    wr,
    cs,
    cr,
    ks,
    kr,
    qs,
    qr,
    hs,
    hr,
    rs,
    rr,
    gs,
    gr,
    ps,
    pr,
):
    sp = lax.axis_index("sp")
    tp = lax.axis_index("tp")
    z, y = lax.div(sp, NY), lax.rem(sp, NY)
    x, core = lax.div(tp, NC), lax.rem(tp, NC)
    partner = x * NC + (1 - core)
    group = y * NTP + tp
    lane = lax.broadcasted_iota(jnp.int32, (1, 128), 1)
    low = lane < 64

    barrier = pltpu.get_barrier_semaphore()

    def greet(dsp, dtp):
        pl.semaphore_signal(
            barrier, inc=1, device_id=(dsp, dtp), device_id_type=pl.DeviceIdType.MESH
        )

    def greet_z(k, c):
        greet(lax.rem(z + k, NZ) * NY + y, tp)
        return c

    def greet_g(k, c):
        g = lax.rem(group + k, NY * NTP)
        greet(z * NY + lax.div(g, NTP), lax.rem(g, NTP))
        return c

    lax.fori_loop(1, NZ, greet_z, 0)
    lax.fori_loop(1, NY * NTP, greet_g, 0)

    loads = [
        (wsh_h, wmod.at[0]),
        (wsc_h, wmod.at[1]),
        (wga_h, wmod.at[2]),
        (ctx_h, ctx),
        (lat_h, lat),
        (wo_h, wo),
        (wk_h, wkv.at[:, pl.ds(0, TOK)]),
        (wv_h, wkv.at[:, pl.ds(TOK, TOK)]),
        (wq_h, wqg.at[:, pl.ds(0, TOK)]),
        (wg_h, wqg.at[:, pl.ds(TOK, TOK)]),
    ]
    loads = [pltpu.make_async_copy(a, b, lsem.at[i]) for i, (a, b) in enumerate(loads)]
    for c in loads:
        c.start()

    for c in loads[:3]:
        c.wait()
    act = act_ref[...]
    sh = dot(act, wmod[0])
    sc = dot(act, wmod[1])
    ga = dot(act, wmod[2])
    zsend[0:2] = sh[0:2, :128]
    zsend[2:4] = sc[0:2, :128]
    zsend[4:6] = sh[0:2, 128:]
    zsend[6:8] = sc[0:2, 128:]
    zsend[8:10] = ga[0:2, :128]
    zsend[10:12] = ga[0:2, 128:]
    zsend[12:16] = jnp.zeros((4, 128), F32)
    zrecv[z] = zsend[...]

    pl.semaphore_wait(barrier, NZ - 1 + NY * NTP - 1)

    def z_copy(k):
        dz = lax.rem(z + k, NZ)
        return remote(zsend, zrecv.at[z], zs.at[dz], zr.at[z], dz * NY + y, tp)

    def z_in(k):
        dz = lax.rem(z + k, NZ)
        return remote(zsend, zrecv.at[dz], zs.at[dz], zr.at[dz], dz * NY + y, tp)

    for k in (4, 3, 5, 2, 6, 1, 7):
        z_copy(k).start()

    loads[5].wait()
    w_copy = remote(wo, wo2, ws, wr, sp, partner)

    loads[3].wait()
    v = ctx[...].astype(F32)
    r = lax.rsqrt(jnp.mean(v * v, axis=1, keepdims=True) + EPSILON)
    rsc[...] = jnp.broadcast_to(r, (CTXL, 128))
    loads[4].wait()

    def lat_stats(i, c):
        rows = pl.ds(pl.multiple_of(i * 32, 32), 32)
        v = lat[rows, :].astype(F32)
        r = lax.rsqrt(jnp.mean(v * v, axis=1, keepdims=True) + EPSILON)
        rsl[rows, :] = jnp.broadcast_to(r, (32, 128))
        return c

    lax.fori_loop(0, TOK // 32, lat_stats, 0)

    for k in range(1, NZ):
        z_in(k).wait_recv()
    total = zrecv[0]
    for k in range(1, NZ):
        total = total + zrecv[k]
    msend[...] = total
    mrecv[y, tp] = total

    def m_copy(k):
        g = lax.rem(group + k, NY * NTP)
        dy, dt = lax.div(g, NTP), lax.rem(g, NTP)
        return remote(msend, mrecv.at[y, tp], ms.at[g], mr.at[group], z * NY + dy, dt)

    def m_in(k):
        g = lax.rem(group + k, NY * NTP)
        dy, dt = lax.div(g, NTP), lax.rem(g, NTP)
        return remote(msend, mrecv.at[dy, dt], ms.at[g], mr.at[g], z * NY + dy, dt)

    def m_start(k, c):
        m_copy(k).start()
        return c

    lax.fori_loop(1, NY * NTP, m_start, 0)
    w_copy.start()

    col = lax.rem(lax.broadcasted_iota(jnp.int32, (64, 128), 1), 64)
    right = lax.div(lax.broadcasted_iota(jnp.int32, (64, 128), 1), 64)
    qcol = lax.broadcasted_iota(jnp.int32, (64, 128), 0)
    first_col = jnp.clip(qcol - WIN_COLS // 2, 0, GRID_W - WIN_COLS)
    in_cols = (col >= first_col) & (col < first_col + WIN_COLS)
    row0 = z * 16

    def table(t, c):
        p = jnp.where(t < 3, t, t + 3)
        base = jnp.clip(row0 + 2 * p - 4, 0, LAST_START)
        for a in range(2):
            row = row0 + 2 * p + a
            off = jnp.clip(row - 4, 0, LAST_START) - base
            d0 = base - row + 7
            for m in range(5):
                line = biasx_ref[y, pl.ds(d0 + 2 * m, 1), :]
                tile = pltpu.roll(
                    jnp.broadcast_to(line, (64, 128)), 113, 1, stride=1, stride_axis=0
                )
                krow = right + 2 * m
                ok = in_cols & (krow >= off) & (krow < off + WIN_ROWS)
                btab[t, a * 64 : a * 64 + 64, m * 128 : m * 128 + 128] = jnp.where(
                    ok, tile, -jnp.inf
                )
        return c

    lax.fori_loop(0, len(SPECIAL), table, 0)

    @pl.when(z == 0)
    def _():
        kvext[0:TOK] = jnp.zeros((TOK, 128), BF16)

    @pl.when(z == NZ - 1)
    def _():
        kvext[5 * TOK : 6 * TOK] = jnp.zeros((TOK, 128), BF16)

    def m_wait(k, c):
        m_in(k).wait_recv()
        return c

    lax.fori_loop(1, NY * NTP, m_wait, 0)
    for t in range(NTP):
        total = mrecv[0, t] + mrecv[1, t] + mrecv[2, t] + mrecv[3, t]
        lo, hi = 256 * t, 256 * t + 128
        mod[0:4, lo : lo + 128] = total[0:4]
        mod[0:4, hi : hi + 128] = total[4:8]
        mod[4:5, lo : lo + 128] = total[8:9]
        mod[4:5, hi : hi + 128] = total[10:11]
    gpre = gpre_ref[...]

    v = ctx[...].astype(F32) * rsc[:, 0:1]
    hidc[...] = (v * (gpre * (1.0 + mod[3:4, :])) + mod[1:2, :]).astype(BF16)
    loads[6].wait()
    loads[7].wait()
    kv = dot(hidc[...], wkv[...])
    for q in range(2):
        kt = kv[:, 128 * q : 128 * q + 128]
        vt = kv[:, 256 + 128 * q : 256 + 128 * q + 128]
        csend[2 * q] = jnp.where(low, kt, half_swap(vt)).astype(BF16)
        csend[2 * q + 1] = jnp.where(low, half_swap(kt), vt).astype(BF16)
    here = pl.ds(pl.multiple_of(sp * CTXL, CTXL), CTXL)
    ctxkv[here, :] = csend[y]

    def c_copy(k):
        d = lax.rem(sp + k, NZ * NY)
        return remote(csend.at[lax.rem(d, NY)], ctxkv.at[here, :], cs.at[d], cr.at[sp], d, tp)

    def c_in(k):
        d = lax.rem(sp + k, NZ * NY)
        there = pl.ds(pl.multiple_of(d * CTXL, CTXL), CTXL)
        return remote(csend.at[y], ctxkv.at[there, :], cs.at[d], cr.at[d], d, tp)

    def c_start(k, c):
        c_copy(k).start()
        return c

    lax.fori_loop(1, NZ * NY, c_start, 0)

    scale = gpre * (1.0 + mod[2:3, :])
    shift = mod[0:1, :]

    def lat_hidden(i, c):
        rows = pl.ds(pl.multiple_of(i * 32, 32), 32)
        v = lat[rows, :].astype(F32) * rsl[rows, 0:1]
        hid[rows, :] = (v * scale + shift).astype(BF16)
        return c

    lax.fori_loop(0, TOK // 32, lat_hidden, 0)
    kv = dot(hid[...], wkv[...])
    for q in range(2):
        kt = kv[:, 128 * q : 128 * q + 128]
        vt = kv[:, 256 + 128 * q : 256 + 128 * q + 128]
        kvsend[2 * q] = jnp.where(low, kt, half_swap(vt)).astype(BF16)
        kvsend[2 * q + 1] = jnp.where(low, half_swap(kt), vt).astype(BF16)
    mine = pl.ds(pl.multiple_of((1 + y) * TOK, TOK), TOK)
    kvext[mine, :] = kvsend[y]

    def k_copy(k):
        dy = lax.rem(y + k, NY)
        return remote(kvsend.at[dy], kvext.at[mine, :], ks.at[dy], kr.at[y], z * NY + dy, tp)

    def k_in(dy):
        rows = pl.ds(pl.multiple_of((1 + dy) * TOK, TOK), TOK)
        return remote(kvsend.at[y], kvext.at[rows, :], ks.at[dy], kr.at[dy], z * NY + dy, tp)

    for k in (2, 1, 3):
        k_copy(k).start()

    loads[8].wait()
    loads[9].wait()
    qg = dot(hid[...], wqg[...])
    for q in range(2):
        qt = qg[:, 128 * q : 128 * q + 128] * (HD**-0.5)
        up, dn = qt[0:128], qt[128:256]
        qsend[2 * q] = jnp.where(low, up, half_swap(dn)).astype(BF16)
        qsend[2 * q + 1] = jnp.where(low, half_swap(up), dn).astype(BF16)
    qrecv[y] = qsend[y]

    def q_copy(k):
        dy = lax.rem(y + k, NY)
        return remote(qsend.at[dy], qrecv.at[y], qs.at[dy], qr.at[y], z * NY + dy, tp)

    def q_in(k):
        dy = lax.rem(y + k, NY)
        return remote(qsend.at[dy], qrecv.at[dy], qs.at[dy], qr.at[dy], z * NY + dy, tp)

    for k in (2, 1, 3):
        q_copy(k).start()
    g = qg[:, 256:].astype(BF16).astype(F32)
    sg[...] = g * (1.0 / (1.0 + jnp.exp(-g)))

    up_src = kvext.at[pl.ds(4 * TOK, TOK), :]
    dn_src = kvext.at[pl.ds(TOK, TOK), :]
    up_dst = kvext.at[pl.ds(0, TOK), :]
    dn_dst = kvext.at[pl.ds(5 * TOK, TOK), :]
    up_copy = remote(up_src, up_dst, hs.at[0], hr.at[0], jnp.minimum(z + 1, NZ - 1) * NY + y, tp)
    dn_copy = remote(dn_src, dn_dst, hs.at[1], hr.at[1], jnp.maximum(z - 1, 0) * NY + y, tp)

    @pl.when(y != 3)
    def _():
        k_in(3).wait_recv()

    @pl.when(z < NZ - 1)
    def _():
        up_copy.start()

    @pl.when(y != 0)
    def _():
        k_in(0).wait_recv()

    @pl.when(z > 0)
    def _():
        dn_copy.start()

    @pl.when(y != 1)
    def _():
        k_in(1).wait_recv()

    @pl.when(y != 2)
    def _():
        k_in(2).wait_recv()

    for k in (1, 2, 3):
        q_in(k).wait_recv()

    def c_wait(k, c):
        c_in(k).wait_recv()
        return c

    lax.fori_loop(1, NZ * NY, c_wait, 0)

    @pl.when(z > 0)
    def _():
        up_copy.wait_recv()

    @pl.when(z < NZ - 1)
    def _():
        dn_copy.wait_recv()

    def r_copy(dy):
        return remote(rsend.at[dy], rrecv.at[y], rs.at[dy], rr.at[y], z * NY + dy, tp)

    def r_in(dy):
        return remote(rsend.at[dy], rrecv.at[dy], rs.at[dy], rr.at[dy], z * NY + dy, tp)

    def block(k, c):
        b = lax.rem(y + k, NY)
        xq = qrecv[b].astype(F32)
        outs = []
        for a in range(2):
            p = 2 * b + a
            xa = xq if a == 0 else half_swap(xq)
            qp = jnp.where(low, xa, 0.0).astype(BF16)
            base = jnp.clip(row0 + 2 * p - 4, 0, LAST_START) - row0 + 4
            rows = pl.ds(pl.multiple_of(base * GRID_W, GRID_W), 10 * GRID_W)
            t = jnp.where(p < 2, p, jnp.where(p < 6, 2, p - 3))
            sc_ctx = dot_nt(qp, ctxkv[...])
            kvw = kvext[rows, :]
            sc_win = dot_nt(qp, kvw) + btab[t]
            top = jnp.maximum(
                jnp.max(sc_ctx, axis=1, keepdims=True), jnp.max(sc_win, axis=1, keepdims=True)
            )
            e_ctx = jnp.exp(sc_ctx - top)
            e_win = jnp.exp(sc_win - top)
            den = jnp.sum(e_ctx, axis=1, keepdims=True) + jnp.sum(e_win, axis=1, keepdims=True)
            o = dot(e_ctx.astype(BF16), ctxkv[...]) + dot(e_win.astype(BF16), kvw)
            outs.append(o * (1.0 / den))
        rsend[b] = jnp.where(low, half_swap(outs[0]), outs[1]).astype(BF16)

        @pl.when(k < NY)
        def _():
            r_copy(b).start()

        @pl.when(k == NY)
        def _():
            rrecv[b] = rsend[b]

        return c

    lax.fori_loop(1, NY + 1, block, 0)
    for k in (1, 2, 3):
        r_in(lax.rem(y + k, NY)).wait_recv()

    for q in range(2):
        x0, x1 = rrecv[2 * q].astype(F32), rrecv[2 * q + 1].astype(F32)
        up = jnp.where(low, x0, half_swap(x1)) * sg[0:128, 128 * q : 128 * q + 128]
        dn = jnp.where(low, half_swap(x0), x1) * sg[128:256, 128 * q : 128 * q + 128]
        cols = slice(128 * q, 128 * q + 128)
        for i in range(2):
            for h in range(2):
                lo = 64 * i + 32 * h
                gated[i, h, :, cols] = up[lo : lo + 32].astype(BF16)
                gated[2 + i, h, :, cols] = dn[lo : lo + 32].astype(BF16)
    g_copy = remote(gated.at[:, 1 - core], grecv, gs, gr, sp, partner)
    g_copy.start()
    w_copy.wait_recv()
    g_copy.wait_recv()
    g_own = gated[:, core].reshape(NX * OUTR, TOK)
    g_other = grecv[...].reshape(NX * OUTR, TOK)
    for n in range(4):
        cols = slice(512 * n, 512 * n + 512)
        term = dot(g_own, wo[:, cols]) + dot(g_other, wo2[:, cols])
        psend[:, :, cols] = term.reshape(NX, OUTR, 512).astype(BF16)

    def p_copy(k):
        dx = lax.rem(x + k, NX)
        return remote(psend.at[dx], precv.at[x], ps.at[dx], pr.at[x], sp, dx * NC + core)

    def p_in(k):
        dx = lax.rem(x + k, NX)
        return remote(psend.at[dx], precv.at[dx], ps.at[dx], pr.at[dx], sp, dx * NC + core)

    for k in (2, 1, 3):
        p_copy(k).start()
    for k in (1, 3, 2):
        p_in(k).wait_recv()
    branch = psend[x].astype(F32)
    for k in (1, 2, 3):
        branch = branch + precv[lax.rem(x + k, NX)].astype(F32)
    branch = branch.astype(BF16).astype(F32)
    normed = branch * lax.rsqrt(jnp.mean(branch * branch, axis=1, keepdims=True) + EPSILON)
    own = lat[pl.ds(pl.multiple_of(tp * OUTR, OUTR), OUTR), :].astype(F32)
    out_ref[...] = (own + mod[4:5, :] * (normed * gpost_ref[...])).astype(BF16)

    for k in range(1, NZ):
        z_copy(k).wait_send()

    def sent(k, c):
        m_copy(k).wait_send()
        c_copy(k).wait_send()
        return c

    lax.fori_loop(1, NY * NTP, sent, 0)
    w_copy.wait_send()
    g_copy.wait_send()
    for k in (1, 2, 3):
        k_copy(k).wait_send()
        q_copy(k).wait_send()
        r_copy(lax.rem(y + k, NY)).wait_send()
        p_copy(k).wait_send()

    @pl.when(z < NZ - 1)
    def _():
        up_copy.wait_send()

    @pl.when(z > 0)
    def _():
        dn_copy.wait_send()


def shards(
    latent,
    context,
    condition,
    context_condition,
    gain_pre,
    gain_post,
    w_shift,
    w_scale,
    w_gate,
    w_query,
    w_key,
    w_value,
    w_silu,
    offset_bias,
    w_out,
):
    sp_index = lax.axis_index("sp")
    in_rows = w_shift.shape[0]
    own = lax.dynamic_slice_in_dim(
        jnp.stack([condition, context_condition]), sp_index * in_rows, in_rows, 1
    )
    act = jnp.pad(jax.nn.silu(own.astype(F32)).astype(BF16), ((0, 6), (0, 0)))
    lines = jnp.pad(offset_bias, ((0, 0), (0, 2), (0, 33)))
    biasx = jnp.concatenate([lines[:, :16], lines[:, 1:17]], axis=2)
    vmem = pl.BlockSpec(memory_space=pltpu.VMEM)
    hbm = pl.BlockSpec(memory_space=pl.ANY)
    dma = pltpu.SemaphoreType.DMA
    return pl.pallas_call(
        kernel,
        name="whole",
        out_shape=jax.ShapeDtypeStruct((OUTR, D), BF16),
        in_specs=[vmem] * 4 + [hbm] * 10,
        out_specs=vmem,
        scratch_shapes=[
            pltpu.VMEM((3, in_rows, TOK), BF16),
            pltpu.VMEM((TOK, D), BF16),
            pltpu.VMEM((CTXL, D), BF16),
            pltpu.VMEM((D, 2 * TOK), BF16),
            pltpu.VMEM((D, 2 * TOK), BF16),
            pltpu.VMEM((TOK, D), BF16),
            pltpu.VMEM((TOK, D), BF16),
            pltpu.VMEM((16, 128), F32),
            pltpu.VMEM((NZ, 16, 128), F32),
            pltpu.VMEM((16, 128), F32),
            pltpu.VMEM((NY, NTP, 16, 128), F32),
            pltpu.VMEM((8, D), F32),
            pltpu.VMEM((len(SPECIAL), 128, 640), F32),
            pltpu.VMEM((TOK, D), BF16),
            pltpu.VMEM((CTXL, D), BF16),
            pltpu.VMEM((TOK, 128), F32),
            pltpu.VMEM((CTXL, 128), F32),
            pltpu.VMEM((NY, CTXL, 128), BF16),
            pltpu.VMEM((CTX, 128), BF16),
            pltpu.VMEM((NY, TOK, 128), BF16),
            pltpu.VMEM((6 * TOK, 128), BF16),
            pltpu.VMEM((NY, 128, 128), BF16),
            pltpu.VMEM((NY, 128, 128), BF16),
            pltpu.VMEM((TOK, TOK), F32),
            pltpu.VMEM((NY, 128, 128), BF16),
            pltpu.VMEM((NY, 128, 128), BF16),
            pltpu.VMEM((NX, NC, OUTR, TOK), BF16),
            pltpu.VMEM((NX, OUTR, TOK), BF16),
            pltpu.VMEM((NX, OUTR, D), BF16),
            pltpu.VMEM((NX, OUTR, D), BF16),
            dma((10,)),
            dma((NZ,)),
            dma((NZ,)),
            dma((NY * NTP,)),
            dma((NY * NTP,)),
            dma,
            dma,
            dma((NZ * NY,)),
            dma((NZ * NY,)),
            dma((NY,)),
            dma((NY,)),
            dma((NY,)),
            dma((NY,)),
            dma((2,)),
            dma((2,)),
            dma((NY,)),
            dma((NY,)),
            dma,
            dma,
            dma((NX,)),
            dma((NX,)),
        ],
        compiler_params=pltpu.CompilerParams(
            collective_id=0, has_side_effects=True, vmem_limit_bytes=48 << 20
        ),
    )(
        act,
        biasx,
        gain_pre.reshape(1, D),
        gain_post.reshape(1, D),
        latent,
        context,
        w_shift,
        w_scale,
        w_gate,
        w_query,
        w_key,
        w_value,
        w_silu,
        w_out,
    )


def solution(mesh):
    in_specs = (
        P("sp", None),
        P("sp", None),
        P(),
        P(),
        P(),
        P(),
        P("sp", "tp"),
        P("sp", "tp"),
        P("sp", "tp"),
        P(None, "tp"),
        P(None, "tp"),
        P(None, "tp"),
        P(None, "tp"),
        P("tp", None, None),
        P("tp", None),
    )
    out_specs = P(("sp", "tp"), None)
    return jax.shard_map(shards, mesh=mesh, in_specs=in_specs, out_specs=out_specs, check_vma=False)
```

time: 144 us -> 61.2 us (0.43)
  the two profiles are of different devices: /device:TPU:32 before, /device:TPU:1 now
where the time goes in v1:
time: 61.2 us; the launch traced here: 60.8 us
  Pallas kernels  52.3 us (85%)
  local copies, waits for them, and re-layouts  8.27 us (14%)
    pallas_call x1, Pallas kernels, shards(): pl.pallas_call(kernel, name='whole', out_shape=jax.ShapeDtypeStruct((OUTR...  52.3 us
    unnamed x30, local copies, waits for them, and re-layouts  8.23 us

profile of v1, /device:TPU:1, one launch (start us, length us, event | category | flops | bytes accessed | tf_op | source)
XLA Modules:
  0.0 60.8 jit_solution(11598258421471600845)
XLA Ops:
  0.0 0.0 copy-start.12
  0.0 0.0 copy-start.13
  0.0 0.0 copy-start.11
  0.0 0.7 %copy-done.12 = bf16[2048]{0:T(1024)(128)(2,1)S(1)} copy-done((bf16[2048]{0:T(1024)(128)(2,1)S(1)}, bf16[2048]{0:T(1024)(128)(2,1)}, u32[]{:S(2)}) %copy-start.12) | copy-done | bytes 4120
  0.7 0.0 copy-done.13
  0.7 0.1 fusion.2
  0.8 0.0 copy-done.11
  0.8 0.0 copy-start.5
  0.9 0.0 copy-start.9
  0.9 0.0 copy-start.10
  0.9 0.0 copy-start.6
  0.9 0.0 copy-start.7
  0.9 0.0 copy-start.8
  0.9 0.1 pad_maximum_fusion.biasx_ref
  1.0 0.7 %copy-done.5 = bf16[32,2048]{1,0:T(8,128)(2,1)S(1)} copy-done((bf16[32,2048]{1,0:T(8,128)(2,1)S(1)}, bf16[32,2048]{1,0:T(8,128)(2,1)}, u32[]{:S(2)}) %copy-start.5) | copy-done | bytes 131096
  1.7 0.0 copy-done.9
  1.7 0.0 copy-done.10
  1.7 0.0 copy-done.6
  1.7 0.0 copy-done.7
  1.7 0.0 copy-done.8
  1.8 0.0 copy-start
  1.8 1.2 %copy-done = bf16[256,2048]{1,0:T(8,128)(2,1)S(1)} copy-done((bf16[256,2048]{1,0:T(8,128)(2,1)S(1)}, bf16[256,2048]{1,0:T(8,128)(2,1)}, u32[]{:S(2)}) %copy-start) | copy-done | bytes 1048600
  3.0 0.0 copy-start.1
  3.0 1.2 %copy-done.1 = bf16[2048,256]{1,0:T(8,128)(2,1)S(1)} copy-done((bf16[2048,256]{1,0:T(8,128)(2,1)S(1)}, bf16[2048,256]{1,0:T(8,128)(2,1)}, u32[]{:S(2)}) %copy-start.1) | copy-done | bytes 1048600
  4.2 0.0 copy-start.2
  4.2 1.2 %copy-done.2 = bf16[2048,256]{1,0:T(8,128)(2,1)S(1)} copy-done((bf16[2048,256]{1,0:T(8,128)(2,1)S(1)}, bf16[2048,256]{1,0:T(8,128)(2,1)}, u32[]{:S(2)}) %copy-start.2) | copy-done | bytes 1048600
  5.4 0.0 copy-start.3
  5.4 1.2 %copy-done.3 = bf16[2048,256]{1,0:T(8,128)(2,1)S(1)} copy-done((bf16[2048,256]{1,0:T(8,128)(2,1)S(1)}, bf16[2048,256]{1,0:T(8,128)(2,1)}, u32[]{:S(2)}) %copy-start.3) | copy-done | bytes 1048600
  6.7 0.0 copy-start.4
  6.7 1.2 %copy-done.4 = bf16[2048,256]{1,0:T(8,128)(2,1)S(1)} copy-done((bf16[2048,256]{1,0:T(8,128)(2,1)S(1)}, bf16[2048,256]{1,0:T(8,128)(2,1)}, u32[]{:S(2)}) %copy-start.4) | copy-done | bytes 1048600
  7.9 52.3 %whole.1 = bf16[32,2048]{1,0:T(8,128)(2,1)S(1)} custom-call(bf16[8,64]{1,0:T(8,128)(2,1)S(1)} %pad.8.act_ref, f32[4,16,128]{2,1,0:T(8,128)S(1)} %pad_maximum_fusion.biasx_ref, f32[1,2048]{1,0:T(1,128)S(1)} %bitcast.2, f32[1,2048]{1,0:T(1,128)S(1)} %bitcast.3, bf16[256,2048]{1,0:T(8,128)(2,1)S(1)} %copy-done, bf16[32,2048]{1,0:T(8,128)(2,1)S(1)} %copy-done.5, ...), custom_call_target="tpu_custom_call" | custom-call | tf_op jit(solution)/shard_map/whole/pallas_call | solution.py:553
  60.2 0.7 %copy.18 = bf16[32,2048]{1,0:T(8,128)(2,1)} copy(bf16[32,2048]{1,0:T(8,128)(2,1)S(1)} %whole.1) | data formatting | bytes 262144
  (5 shorter events, 0.0 us)
Async XLA Ops:
  0.0 0.7 %copy-start.12 = (bf16[2048]{0:T(1024)(128)(2,1)S(1)}, bf16[2048]{0:T(1024)(128)(2,1)}, u32[]{:S(2)}) copy-start(bf16[2048]{0:T(1024)(128)(2,1)} %param.17) | copy-start | bytes 12292
  0.0 0.7 %copy-start.13 = (bf16[2048]{0:T(1024)(128)(2,1)S(1)}, bf16[2048]{0:T(1024)(128)(2,1)}, u32[]{:S(2)}) copy-start(bf16[2048]{0:T(1024)(128)(2,1)} %param.18) | copy-start | bytes 12292
  0.0 0.8 %copy-start.11 = (f32[4,15,31]{2,0,1:T(4,128)S(1)}, f32[4,15,31]{2,0,1:T(4,128)}, u32[]{:S(2)}) copy-start(f32[4,15,31]{2,0,1:T(4,128)} %param.28) | copy-start | bytes 22324
  0.8 0.9 %copy-start.5 = (bf16[32,2048]{1,0:T(8,128)(2,1)S(1)}, bf16[32,2048]{1,0:T(8,128)(2,1)}, u32[]{:S(2)}) copy-start(bf16[32,2048]{1,0:T(8,128)(2,1)} %ctx_h.1) | copy-start | bytes 393220
  0.9 0.9 %copy-start.9 = (f32[2048]{0:T(1024)S(1)}, f32[2048]{0:T(1024)}, u32[]{:S(2)}) copy-start(f32[2048]{0:T(1024)} %param.19) | copy-start | bytes 24580
  0.9 0.9 %copy-start.10 = (f32[2048]{0:T(1024)S(1)}, f32[2048]{0:T(1024)}, u32[]{:S(2)}) copy-start(f32[2048]{0:T(1024)} %param.20) | copy-start | bytes 24580
  0.9 0.8 %copy-start.6 = (bf16[64,256]{1,0:T(8,128)(2,1)S(1)}, bf16[64,256]{1,0:T(8,128)(2,1)}, u32[]{:S(2)}) copy-start(bf16[64,256]{1,0:T(8,128)(2,1)} %wsh_h.1) | copy-start | bytes 98308
  0.9 0.8 %copy-start.7 = (bf16[64,256]{1,0:T(8,128)(2,1)S(1)}, bf16[64,256]{1,0:T(8,128)(2,1)}, u32[]{:S(2)}) copy-start(bf16[64,256]{1,0:T(8,128)(2,1)} %wsc_h.1) | copy-start | bytes 98308
  0.9 0.8 %copy-start.8 = (bf16[64,256]{1,0:T(8,128)(2,1)S(1)}, bf16[64,256]{1,0:T(8,128)(2,1)}, u32[]{:S(2)}) copy-start(bf16[64,256]{1,0:T(8,128)(2,1)} %wga_h.1) | copy-start | bytes 98308
  1.8 1.2 %copy-start = (bf16[256,2048]{1,0:T(8,128)(2,1)S(1)}, bf16[256,2048]{1,0:T(8,128)(2,1)}, u32[]{:S(2)}) copy-start(bf16[256,2048]{1,0:T(8,128)(2,1)} %lat_h.1) | copy-start | bytes 3145732
  3.0 1.2 %copy-start.1 = (bf16[2048,256]{1,0:T(8,128)(2,1)S(1)}, bf16[2048,256]{1,0:T(8,128)(2,1)}, u32[]{:S(2)}) copy-start(bf16[2048,256]{1,0:T(8,128)(2,1)} %wq_h.1) | copy-start | bytes 3145732
  4.2 1.2 %copy-start.2 = (bf16[2048,256]{1,0:T(8,128)(2,1)S(1)}, bf16[2048,256]{1,0:T(8,128)(2,1)}, u32[]{:S(2)}) copy-start(bf16[2048,256]{1,0:T(8,128)(2,1)} %wk_h.1) | copy-start | bytes 3145732
  5.4 1.2 %copy-start.3 = (bf16[2048,256]{1,0:T(8,128)(2,1)S(1)}, bf16[2048,256]{1,0:T(8,128)(2,1)}, u32[]{:S(2)}) copy-start(bf16[2048,256]{1,0:T(8,128)(2,1)} %wv_h.1) | copy-start | bytes 3145732
  6.7 1.2 %copy-start.4 = (bf16[2048,256]{1,0:T(8,128)(2,1)S(1)}, bf16[2048,256]{1,0:T(8,128)(2,1)}, u32[]{:S(2)}) copy-start(bf16[2048,256]{1,0:T(8,128)(2,1)} %wg_h.1) | copy-start | bytes 3145732

commit v2 on v1

--- a/solution.py
+++ b/solution.py
@@ -45,15 +45,29 @@
     )
 
 
+class Phases:
+    def __init__(self):
+        self.scope = None
+
+    def __call__(self, name):
+        if self.scope is not None:
+            self.scope.__exit__(None, None, None)
+        self.scope = None
+        if name:
+            self.scope = jax.named_scope(name)
+            self.scope.__enter__()
+
+
 def half_swap(v):
     return pltpu.roll(v, 64, 1)
 
 
 def kernel(
-    act_ref,
-    biasx_ref,
-    gpre_ref,
-    gpost_ref,
+    cond_h,
+    cond2_h,
+    gpre_h,
+    gpost_h,
+    bias_h,
     lat_h,
     ctx_h,
     wsh_h,
@@ -65,9 +79,13 @@
     wg_h,
     wo_h,
     out_ref,
+    conds,
+    condf,
+    gains,
+    bias,
+    biasx,
     wmod,
     lat,
-    ctx,
     wkv,
     wqg,
     wo,
@@ -76,12 +94,14 @@
     zrecv,
     msend,
     mrecv,
+    zgsend,
+    zgrecv,
+    mgsend,
+    mgrecv,
     mod,
     btab,
     hid,
-    hidc,
     rsl,
-    rsc,
     csend,
     ctxkv,
     kvsend,
@@ -100,6 +120,10 @@
     zr,
     ms,
     mr,
+    zgs,
+    zgr,
+    mgs,
+    mgr,
     ws,
     wr,
     cs,
@@ -126,31 +150,19 @@
     lane = lax.broadcasted_iota(jnp.int32, (1, 128), 1)
     low = lane < 64
 
-    barrier = pltpu.get_barrier_semaphore()
-
-    def greet(dsp, dtp):
-        pl.semaphore_signal(
-            barrier, inc=1, device_id=(dsp, dtp), device_id_type=pl.DeviceIdType.MESH
-        )
-
-    def greet_z(k, c):
-        greet(lax.rem(z + k, NZ) * NY + y, tp)
-        return c
-
-    def greet_g(k, c):
-        g = lax.rem(group + k, NY * NTP)
-        greet(z * NY + lax.div(g, NTP), lax.rem(g, NTP))
-        return c
-
-    lax.fori_loop(1, NZ, greet_z, 0)
-    lax.fori_loop(1, NY * NTP, greet_g, 0)
-
+    phase = Phases()
+    phase("loads")
     loads = [
+        (cond_h, conds.at[0]),
+        (cond2_h, conds.at[1]),
         (wsh_h, wmod.at[0]),
         (wsc_h, wmod.at[1]),
         (wga_h, wmod.at[2]),
-        (ctx_h, ctx),
-        (lat_h, lat),
+        (ctx_h, lat.at[pl.ds(TOK, CTXL), :]),
+        (lat_h, lat.at[pl.ds(0, TOK), :]),
+        (gpre_h, gains.at[0]),
+        (gpost_h, gains.at[1]),
+        (bias_h, bias),
         (wo_h, wo),
         (wk_h, wkv.at[:, pl.ds(0, TOK)]),
         (wv_h, wkv.at[:, pl.ds(TOK, TOK)]),
@@ -161,9 +173,36 @@
     for c in loads:
         c.start()
 
-    for c in loads[:3]:
+    phase("greet")
+    barrier = pltpu.get_barrier_semaphore()
+
+    def greet(dsp, dtp):
+        pl.semaphore_signal(
+            barrier, inc=1, device_id=(dsp, dtp), device_id_type=pl.DeviceIdType.MESH
+        )
+
+    def greet_z(k, c):
+        greet(lax.rem(z + k, NZ) * NY + y, tp)
+        return c
+
+    def greet_g(k, c):
+        g = lax.rem(group + k, NY * NTP)
+        greet(z * NY + lax.div(g, NTP), lax.rem(g, NTP))
+        return c
+
+    lax.fori_loop(1, NZ, greet_z, 0)
+    lax.fori_loop(1, NY * NTP, greet_g, 0)
+
+    phase("partial")
+    for c in loads[:2]:
         c.wait()
-    act = act_ref[...]
+    v = conds[...].astype(F32)
+    condf[...] = v * (1.0 / (1.0 + jnp.exp(-v)))
+    line = jnp.concatenate([condf[i, pl.ds(lax.div(sp, 2), 1), :] for i in range(2)], axis=0)
+    line = jnp.where(lax.rem(sp, 2) == 1, half_swap(line), line)[:, :64]
+    act = jnp.concatenate([line, jnp.zeros((6, 64), F32)], axis=0).astype(BF16)
+    for c in loads[2:5]:
+        c.wait()
     sh = dot(act, wmod[0])
     sc = dot(act, wmod[1])
     ga = dot(act, wmod[2])
@@ -171,13 +210,15 @@
     zsend[2:4] = sc[0:2, :128]
     zsend[4:6] = sh[0:2, 128:]
     zsend[6:8] = sc[0:2, 128:]
-    zsend[8:10] = ga[0:2, :128]
-    zsend[10:12] = ga[0:2, 128:]
-    zsend[12:16] = jnp.zeros((4, 128), F32)
+    zgsend[0:1] = ga[0:1, :128]
+    zgsend[1:2] = ga[0:1, 128:]
     zrecv[z] = zsend[...]
-
+    zgrecv[z] = zgsend[...]
+
+    phase("barrier")
     pl.semaphore_wait(barrier, NZ - 1 + NY * NTP - 1)
 
+    phase("z_start")
     def z_copy(k):
         dz = lax.rem(z + k, NZ)
         return remote(zsend, zrecv.at[z], zs.at[dz], zr.at[z], dz * NY + y, tp)
@@ -186,29 +227,52 @@
         dz = lax.rem(z + k, NZ)
         return remote(zsend, zrecv.at[dz], zs.at[dz], zr.at[dz], dz * NY + y, tp)
 
-    for k in (4, 3, 5, 2, 6, 1, 7):
+    def zg_copy(k):
+        dz = lax.rem(z + k, NZ)
+        return remote(zgsend, zgrecv.at[z], zgs.at[dz], zgr.at[z], dz * NY + y, tp)
+
+    def zg_in(k):
+        dz = lax.rem(z + k, NZ)
+        return remote(zgsend, zgrecv.at[dz], zgs.at[dz], zgr.at[dz], dz * NY + y, tp)
+
+    far_first = (4, 3, 5, 2, 6, 1, 7)
+    for k in far_first:
         z_copy(k).start()
+    for k in far_first:
+        zg_copy(k).start()
+
+    phase("stats")
+    w_copy = remote(wo, wo2, ws, wr, sp, partner)
 
     loads[5].wait()
-    w_copy = remote(wo, wo2, ws, wr, sp, partner)
-
-    loads[3].wait()
-    v = ctx[...].astype(F32)
-    r = lax.rsqrt(jnp.mean(v * v, axis=1, keepdims=True) + EPSILON)
-    rsc[...] = jnp.broadcast_to(r, (CTXL, 128))
-    loads[4].wait()
-
-    def lat_stats(i, c):
+    loads[6].wait()
+
+    def row_stats(i, c):
         rows = pl.ds(pl.multiple_of(i * 32, 32), 32)
         v = lat[rows, :].astype(F32)
         r = lax.rsqrt(jnp.mean(v * v, axis=1, keepdims=True) + EPSILON)
         rsl[rows, :] = jnp.broadcast_to(r, (32, 128))
         return c
 
-    lax.fori_loop(0, TOK // 32, lat_stats, 0)
-
+    lax.fori_loop(0, (TOK + CTXL) // 32, row_stats, 0)
+    loads[7].wait()
+    loads[8].wait()
+    for t in range(16):
+        mod[5:6, 128 * t : 128 * t + 128] = gains[0, t : t + 1, :]
+        mod[6:7, 128 * t : 128 * t + 128] = gains[1, t : t + 1, :]
+    loads[9].wait()
+    biasx[...] = jnp.zeros((16, 128), F32)
+    for d in range(2 * WIN_ROWS - 1):
+        line = bias[d, pl.ds(y, 1), :]
+        biasx[d : d + 1, 0:31] = line
+        if d > 0:
+            biasx[d - 1 : d, 64:95] = line
+    loads[10].wait()
+
+    phase("z_wait")
     for k in range(1, NZ):
         z_in(k).wait_recv()
+    phase("m_start")
     total = zrecv[0]
     for k in range(1, NZ):
         total = total + zrecv[k]
@@ -232,6 +296,7 @@
     lax.fori_loop(1, NY * NTP, m_start, 0)
     w_copy.start()
 
+    phase("tables")
     col = lax.rem(lax.broadcasted_iota(jnp.int32, (64, 128), 1), 64)
     right = lax.div(lax.broadcasted_iota(jnp.int32, (64, 128), 1), 64)
     qcol = lax.broadcasted_iota(jnp.int32, (64, 128), 0)
@@ -247,7 +312,7 @@
             off = jnp.clip(row - 4, 0, LAST_START) - base
             d0 = base - row + 7
             for m in range(5):
-                line = biasx_ref[y, pl.ds(d0 + 2 * m, 1), :]
+                line = biasx[pl.ds(d0 + 2 * m, 1), :]
                 tile = pltpu.roll(
                     jnp.broadcast_to(line, (64, 128)), 113, 1, stride=1, stride_axis=0
                 )
@@ -272,21 +337,33 @@
         m_in(k).wait_recv()
         return c
 
+    phase("m_wait")
     lax.fori_loop(1, NY * NTP, m_wait, 0)
+    phase("mod")
     for t in range(NTP):
         total = mrecv[0, t] + mrecv[1, t] + mrecv[2, t] + mrecv[3, t]
         lo, hi = 256 * t, 256 * t + 128
         mod[0:4, lo : lo + 128] = total[0:4]
         mod[0:4, hi : hi + 128] = total[4:8]
-        mod[4:5, lo : lo + 128] = total[8:9]
-        mod[4:5, hi : hi + 128] = total[10:11]
-    gpre = gpre_ref[...]
-
-    v = ctx[...].astype(F32) * rsc[:, 0:1]
-    hidc[...] = (v * (gpre * (1.0 + mod[3:4, :])) + mod[1:2, :]).astype(BF16)
-    loads[6].wait()
-    loads[7].wait()
-    kv = dot(hidc[...], wkv[...])
+    mod[2:3, :] = mod[5:6, :] * (1.0 + mod[2:3, :])
+    mod[3:4, :] = mod[5:6, :] * (1.0 + mod[3:4, :])
+
+    phase("hidden")
+    def hidden(rows, which):
+        v = lat[rows, :].astype(F32) * rsl[rows, 0:1]
+        hid[rows, :] = (v * mod[2 + which : 3 + which, :] + mod[which : 1 + which, :]).astype(BF16)
+
+    def lat_hidden(i, c):
+        hidden(pl.ds(pl.multiple_of(i * 32, 32), 32), 0)
+        return c
+
+    hidden(pl.ds(TOK, CTXL), 1)
+    lax.fori_loop(0, TOK // 32, lat_hidden, 0)
+    phase("kv")
+    loads[11].wait()
+    loads[12].wait()
+    kv_all = dot(hid[...], wkv[...])
+    kv = kv_all[TOK:]
     for q in range(2):
         kt = kv[:, 128 * q : 128 * q + 128]
         vt = kv[:, 256 + 128 * q : 256 + 128 * q + 128]
@@ -310,17 +387,7 @@
 
     lax.fori_loop(1, NZ * NY, c_start, 0)
 
-    scale = gpre * (1.0 + mod[2:3, :])
-    shift = mod[0:1, :]
-
-    def lat_hidden(i, c):
-        rows = pl.ds(pl.multiple_of(i * 32, 32), 32)
-        v = lat[rows, :].astype(F32) * rsl[rows, 0:1]
-        hid[rows, :] = (v * scale + shift).astype(BF16)
-        return c
-
-    lax.fori_loop(0, TOK // 32, lat_hidden, 0)
-    kv = dot(hid[...], wkv[...])
+    kv = kv_all[:TOK]
     for q in range(2):
         kt = kv[:, 128 * q : 128 * q + 128]
         vt = kv[:, 256 + 128 * q : 256 + 128 * q + 128]
@@ -340,9 +407,9 @@
     for k in (2, 1, 3):
         k_copy(k).start()
 
-    loads[8].wait()
-    loads[9].wait()
-    qg = dot(hid[...], wqg[...])
+    phase("qg")
+    loads[13].wait()
+    qg = dot(hid[0:TOK, :], wqg[:, 0:TOK])
     for q in range(2):
         qt = qg[:, 128 * q : 128 * q + 128] * (HD**-0.5)
         up, dn = qt[0:128], qt[128:256]
@@ -360,8 +427,35 @@
 
     for k in (2, 1, 3):
         q_copy(k).start()
-    g = qg[:, 256:].astype(BF16).astype(F32)
+    phase("g")
+    loads[14].wait()
+    g = dot(hid[0:TOK, :], wqg[:, TOK:]).astype(BF16).astype(F32)
     sg[...] = g * (1.0 / (1.0 + jnp.exp(-g)))
+
+    phase("kq_wait")
+    for k in range(1, NZ):
+        zg_in(k).wait_recv()
+    total = zgrecv[0]
+    for k in range(1, NZ):
+        total = total + zgrecv[k]
+    mgsend[...] = total
+    mgrecv[y, tp] = total
+
+    def mg_copy(k):
+        g = lax.rem(group + k, NY * NTP)
+        dy, dt = lax.div(g, NTP), lax.rem(g, NTP)
+        return remote(mgsend, mgrecv.at[y, tp], mgs.at[g], mgr.at[group], z * NY + dy, dt)
+
+    def mg_in(k):
+        g = lax.rem(group + k, NY * NTP)
+        dy, dt = lax.div(g, NTP), lax.rem(g, NTP)
+        return remote(mgsend, mgrecv.at[dy, dt], mgs.at[g], mgr.at[g], z * NY + dy, dt)
+
+    def mg_start(k, c):
+        mg_copy(k).start()
+        return c
+
+    lax.fori_loop(1, NY * NTP, mg_start, 0)
 
     up_src = kvext.at[pl.ds(4 * TOK, TOK), :]
     dn_src = kvext.at[pl.ds(TOK, TOK), :]
@@ -397,12 +491,14 @@
     for k in (1, 2, 3):
         q_in(k).wait_recv()
 
+    phase("c_wait")
     def c_wait(k, c):
         c_in(k).wait_recv()
         return c
 
     lax.fori_loop(1, NZ * NY, c_wait, 0)
 
+    phase("h_wait")
     @pl.when(z > 0)
     def _():
         up_copy.wait_recv()
@@ -411,6 +507,7 @@
     def _():
         dn_copy.wait_recv()
 
+    phase("attention")
     def r_copy(dy):
         return remote(rsend.at[dy], rrecv.at[y], rs.at[dy], rr.at[y], z * NY + dy, tp)
 
@@ -452,9 +549,11 @@
         return c
 
     lax.fori_loop(1, NY + 1, block, 0)
+    phase("r_wait")
     for k in (1, 2, 3):
         r_in(lax.rem(y + k, NY)).wait_recv()
 
+    phase("gate")
     for q in range(2):
         x0, x1 = rrecv[2 * q].astype(F32), rrecv[2 * q + 1].astype(F32)
         up = jnp.where(low, x0, half_swap(x1)) * sg[0:128, 128 * q : 128 * q + 128]
@@ -467,8 +566,10 @@
                 gated[2 + i, h, :, cols] = dn[lo : lo + 32].astype(BF16)
     g_copy = remote(gated.at[:, 1 - core], grecv, gs, gr, sp, partner)
     g_copy.start()
+    phase("g_wait")
     w_copy.wait_recv()
     g_copy.wait_recv()
+    phase("project")
     g_own = gated[:, core].reshape(NX * OUTR, TOK)
     g_other = grecv[...].reshape(NX * OUTR, TOK)
     for n in range(4):
@@ -486,22 +587,16 @@
 
     for k in (2, 1, 3):
         p_copy(k).start()
-    for k in (1, 3, 2):
-        p_in(k).wait_recv()
-    branch = psend[x].astype(F32)
-    for k in (1, 2, 3):
-        branch = branch + precv[lax.rem(x + k, NX)].astype(F32)
-    branch = branch.astype(BF16).astype(F32)
-    normed = branch * lax.rsqrt(jnp.mean(branch * branch, axis=1, keepdims=True) + EPSILON)
-    own = lat[pl.ds(pl.multiple_of(tp * OUTR, OUTR), OUTR), :].astype(F32)
-    out_ref[...] = (own + mod[4:5, :] * (normed * gpost_ref[...])).astype(BF16)
-
+    phase("sent1")
     for k in range(1, NZ):
         z_copy(k).wait_send()
+        zg_copy(k).wait_send()
 
     def sent(k, c):
         m_copy(k).wait_send()
+        mg_copy(k).wait_send()
         c_copy(k).wait_send()
+        mg_in(k).wait_recv()
         return c
 
     lax.fori_loop(1, NY * NTP, sent, 0)
@@ -511,15 +606,38 @@
         k_copy(k).wait_send()
         q_copy(k).wait_send()
         r_copy(lax.rem(y + k, NY)).wait_send()
+
+    @pl.when(z < NZ - 1)
+    def _():
+        up_copy.wait_send()
+
+    @pl.when(z > 0)
+    def _():
+        dn_copy.wait_send()
+
+    for t in range(NTP):
+        total = mgrecv[0, t] + mgrecv[1, t] + mgrecv[2, t] + mgrecv[3, t]
+        mod[4:5, 256 * t : 256 * t + 128] = total[0:1]
+        mod[4:5, 256 * t + 128 : 256 * t + 256] = total[1:2]
+    phase("p_wait1")
+    p_in(1).wait_recv()
+    phase("p_wait3")
+    p_in(3).wait_recv()
+    phase("p_wait2")
+    p_in(2).wait_recv()
+    phase("final")
+    branch = psend[x].astype(F32)
+    for k in (1, 2, 3):
+        branch = branch + precv[lax.rem(x + k, NX)].astype(F32)
+    branch = branch.astype(BF16).astype(F32)
+    normed = branch * lax.rsqrt(jnp.mean(branch * branch, axis=1, keepdims=True) + EPSILON)
+    own = lat[pl.ds(pl.multiple_of(tp * OUTR, OUTR), OUTR), :].astype(F32)
+    out_ref[...] = (own + mod[4:5, :] * (normed * mod[6:7, :])).astype(BF16)
+
+    phase("sent")
+    for k in (1, 2, 3):
         p_copy(k).wait_send()
-
-    @pl.when(z < NZ - 1)
-    def _():
-        up_copy.wait_send()
-
-    @pl.when(z > 0)
-    def _():
-        dn_copy.wait_send()
+    phase(None)
 
 
 def shards(
@@ -539,41 +657,40 @@
     offset_bias,
     w_out,
 ):
-    sp_index = lax.axis_index("sp")
     in_rows = w_shift.shape[0]
-    own = lax.dynamic_slice_in_dim(
-        jnp.stack([condition, context_condition]), sp_index * in_rows, in_rows, 1
-    )
-    act = jnp.pad(jax.nn.silu(own.astype(F32)).astype(BF16), ((0, 6), (0, 0)))
-    lines = jnp.pad(offset_bias, ((0, 0), (0, 2), (0, 33)))
-    biasx = jnp.concatenate([lines[:, :16], lines[:, 1:17]], axis=2)
     vmem = pl.BlockSpec(memory_space=pltpu.VMEM)
-    hbm = pl.BlockSpec(memory_space=pl.ANY)
+    hbm = pl.BlockSpec(memory_space=pltpu.HBM)
     dma = pltpu.SemaphoreType.DMA
     return pl.pallas_call(
         kernel,
         name="whole",
         out_shape=jax.ShapeDtypeStruct((OUTR, D), BF16),
-        in_specs=[vmem] * 4 + [hbm] * 10,
+        in_specs=[hbm] * 15,
         out_specs=vmem,
         scratch_shapes=[
+            pltpu.VMEM((2, 16, 128), BF16),
+            pltpu.VMEM((2, 16, 128), F32),
+            pltpu.VMEM((2, 16, 128), F32),
+            pltpu.VMEM((2 * WIN_ROWS - 1, NY, 2 * WIN_COLS - 1), F32),
+            pltpu.VMEM((16, 128), F32),
             pltpu.VMEM((3, in_rows, TOK), BF16),
-            pltpu.VMEM((TOK, D), BF16),
-            pltpu.VMEM((CTXL, D), BF16),
+            pltpu.VMEM((TOK + CTXL, D), BF16),
             pltpu.VMEM((D, 2 * TOK), BF16),
             pltpu.VMEM((D, 2 * TOK), BF16),
             pltpu.VMEM((TOK, D), BF16),
             pltpu.VMEM((TOK, D), BF16),
-            pltpu.VMEM((16, 128), F32),
-            pltpu.VMEM((NZ, 16, 128), F32),
-            pltpu.VMEM((16, 128), F32),
-            pltpu.VMEM((NY, NTP, 16, 128), F32),
+            pltpu.VMEM((8, 128), F32),
+            pltpu.VMEM((NZ, 8, 128), F32),
+            pltpu.VMEM((8, 128), F32),
+            pltpu.VMEM((NY, NTP, 8, 128), F32),
+            pltpu.VMEM((2, 128), F32),
+            pltpu.VMEM((NZ, 2, 128), F32),
+            pltpu.VMEM((2, 128), F32),
+            pltpu.VMEM((NY, NTP, 2, 128), F32),
             pltpu.VMEM((8, D), F32),
             pltpu.VMEM((len(SPECIAL), 128, 640), F32),
-            pltpu.VMEM((TOK, D), BF16),
-            pltpu.VMEM((CTXL, D), BF16),
-            pltpu.VMEM((TOK, 128), F32),
-            pltpu.VMEM((CTXL, 128), F32),
+            pltpu.VMEM((TOK + CTXL, D), BF16),
+            pltpu.VMEM((TOK + CTXL, 128), F32),
             pltpu.VMEM((NY, CTXL, 128), BF16),
             pltpu.VMEM((CTX, 128), BF16),
             pltpu.VMEM((NY, TOK, 128), BF16),
@@ -587,7 +704,11 @@
             pltpu.VMEM((NX, OUTR, TOK), BF16),
             pltpu.VMEM((NX, OUTR, D), BF16),
             pltpu.VMEM((NX, OUTR, D), BF16),
-            dma((10,)),
+            dma((15,)),
+            dma((NZ,)),
+            dma((NZ,)),
+            dma((NY * NTP,)),
+            dma((NY * NTP,)),
             dma((NZ,)),
             dma((NZ,)),
             dma((NY * NTP,)),
@@ -610,13 +731,14 @@
             dma((NX,)),
         ],
         compiler_params=pltpu.CompilerParams(
-            collective_id=0, has_side_effects=True, vmem_limit_bytes=48 << 20
+            collective_id=0, has_side_effects=True, vmem_limit_bytes=67043328
         ),
     )(
-        act,
-        biasx,
-        gain_pre.reshape(1, D),
-        gain_post.reshape(1, D),
+        condition.reshape(16, 128),
+        context_condition.reshape(16, 128),
+        gain_pre.reshape(16, 128),
+        gain_post.reshape(16, 128),
+        jnp.transpose(offset_bias, (1, 0, 2)),
         latent,
         context,
         w_shift,

time: 61.2 us -> 55 us (0.90)
  local copies, waits for them, and re-layouts: 8.27 us -> 1.57 us
  Pallas kernels: 52.3 us -> 53.3 us
    unnamed x30 -> x1, local copies, waits for them, and re-layouts: 8.23 us -> 1.57 us
    pallas_call x1, Pallas kernels: 52.3 us -> 53.3 us  [shards(): pl.pallas_call(kernel, name='whole', out_shape=jax.ShapeDtypeStruct((OUTR...]
where the time goes in v2:
time: 55 us; the launch traced here: 54.9 us
  Pallas kernels  53.3 us (97%)
  local copies, waits for them, and re-layouts  1.57 us (3%)
    pallas_call x1, Pallas kernels, shards(): pl.pallas_call(kernel, name='whole', out_shape=jax.ShapeDtypeStruct((OUTR...  53.3 us
    unnamed x1, local copies, waits for them, and re-layouts  1.57 us

profile of v2, /device:TPU:1, one launch (start us, length us, event | category | flops | bytes accessed | tf_op | source)
XLA Modules:
  0.0 54.9 jit_solution(2555259754419874789)
XLA Ops:
  0.0 53.3 %whole.1 = bf16[32,2048]{1,0:T(8,128)(2,1)} custom-call(bf16[16,128]{1,0:T(8,128)(2,1)} %bitcast.8, bf16[16,128]{1,0:T(8,128)(2,1)} %bitcast.9, f32[16,128]{1,0:T(8,128)} %bitcast.6, f32[16,128]{1,0:T(8,128)} %bitcast.7, f32[15,4,31]{2,1,0:T(4,128)} %bitcast.5, bf16[256,2048]{1,0:T(8,128)(2,1)} %lat_h.1, bf16[32,2048]{1,0:T(8,128)(2,1)} %ctx_h.1, ...), custom_call_target="tpu_custom_call" | custom-call | tf_op jit(solution)/shard_map/whole/pallas_call | solution.py:664
  53.3 1.6 %copy.17 = bf16[32,2048]{1,0:T(8,128)(2,1)} copy(bf16[32,2048]{1,0:T(8,128)(2,1)} %whole.1) | data formatting | bytes 262144

commit v3 on v2

v3 whole, which is shorter than its diff:
```python
import functools

import jax
import jax.numpy as jnp
from jax import lax
from jax.experimental import pallas as pl
from jax.experimental.pallas import tpu as pltpu
from jax.sharding import PartitionSpec as P

GRID_W = 64
WIN_ROWS = 8
WIN_COLS = 16
EPSILON = 1e-06
NZ, NY, NX, NC = 8, 4, 4, 2
NTP = NX * NC
D = 2048
HD = 64
TOK = 256
CTXL = 32
CTX = 1024
OUTR = TOK // NTP
LAST_START = NZ * NY * TOK // GRID_W - WIN_ROWS
SPECIAL = (0, 1, 2, 6, 7)
F32 = jnp.float32
BF16 = jnp.bfloat16
NT = (((1,), (1,)), ((), ()))


def dot(a, b):
    return jnp.dot(a, b, preferred_element_type=F32)


def dot_nt(a, b):
    return lax.dot_general(a, b, NT, preferred_element_type=F32)


def remote(src, dst, ssem, rsem, sp, tp):
    return pltpu.make_async_remote_copy(
        src_ref=src,
        dst_ref=dst,
        send_sem=ssem,
        recv_sem=rsem,
        device_id=(sp, tp),
        device_id_type=pl.DeviceIdType.MESH,
    )


class Phases:
    def __init__(self):
        self.scope = None

    def __call__(self, name):
        if self.scope is not None:
            self.scope.__exit__(None, None, None)
        self.scope = None
        if name:
            self.scope = jax.named_scope(name)
            self.scope.__enter__()


def drain(ref, sem):
    pltpu.make_async_copy(ref, ref, sem).wait()


def half_swap(v):
    return pltpu.roll(v, 64, 1)


def kernel(
    cond_h,
    cond2_h,
    gpre_h,
    gpost_h,
    bias_h,
    lat_h,
    ctx_h,
    wsh_h,
    wsc_h,
    wga_h,
    wq_h,
    wk_h,
    wv_h,
    wg_h,
    wo_h,
    out_ref,
    conds,
    condf,
    gains,
    bias,
    biasx,
    wmod,
    lat,
    wkv,
    wqg,
    wo,
    wo2,
    zsend,
    zrecv,
    msend,
    mrecv,
    zgsend,
    zgrecv,
    mgsend,
    mgrecv,
    mod,
    btab,
    hid,
    rsl,
    csend,
    ctxkv,
    kvsend,
    kvext,
    qsend,
    qrecv,
    gbuf,
    gother,
    sgate,
    rsend,
    rrecv,
    gated,
    psend,
    precv,
    lsem,
    zs,
    zr,
    ms,
    mr,
    zgs,
    zgr,
    mgs,
    mgr,
    ws,
    wr,
    cs,
    cr,
    ks,
    kr,
    qs,
    qr,
    hs,
    hr,
    rs,
    rr,
    gs,
    gr,
    ps,
    pr,
):
    sp = lax.axis_index("sp")
    tp = lax.axis_index("tp")
    z, y = lax.div(sp, NY), lax.rem(sp, NY)
    x, core = lax.div(tp, NC), lax.rem(tp, NC)
    partner = x * NC + (1 - core)
    group = y * NTP + tp
    lane = lax.broadcasted_iota(jnp.int32, (1, 128), 1)
    low = lane < 64

    phase = Phases()
    phase("loads")
    def load(sem, *moves):
        for a, b in moves:
            pltpu.make_async_copy(a, b, lsem.at[sem]).start()

    load(0, (cond_h, conds.at[0]), (cond2_h, conds.at[1]))
    load(1, (wsh_h, wmod.at[0]), (wsc_h, wmod.at[1]), (wga_h, wmod.at[2]))
    load(2, (ctx_h, lat.at[pl.ds(TOK, CTXL), :]), (lat_h, lat.at[pl.ds(0, TOK), :]))
    load(3, (gpre_h, gains.at[0]), (gpost_h, gains.at[1]))
    load(4, (bias_h, bias))
    load(5, (wo_h, wo))
    load(6, (wk_h, wkv.at[:, pl.ds(0, TOK)]), (wv_h, wkv.at[:, pl.ds(TOK, TOK)]))
    load(7, (wq_h, wqg.at[:, pl.ds(0, TOK)]), (wg_h, wqg.at[:, pl.ds(TOK, TOK)]))

    phase("greet")
    barrier = pltpu.get_barrier_semaphore()

    def greet(dsp, dtp):
        pl.semaphore_signal(
            barrier, inc=1, device_id=(dsp, dtp), device_id_type=pl.DeviceIdType.MESH
        )

    def greet_z(k, c):
        greet(lax.rem(z + k, NZ) * NY + y, tp)
        return c

    def greet_g(k, c):
        g = lax.rem(group + k, NY * NTP)
        greet(z * NY + lax.div(g, NTP), lax.rem(g, NTP))
        return c

    lax.fori_loop(1, NZ, greet_z, 0)
    lax.fori_loop(1, NY * NTP, greet_g, 0)

    phase("partial")
    drain(conds, lsem.at[0])
    v = conds[...].astype(F32)
    condf[...] = v * (1.0 / (1.0 + jnp.exp(-v)))
    line = jnp.concatenate([condf[i, pl.ds(lax.div(sp, 2), 1), :] for i in range(2)], axis=0)
    line = jnp.where(lax.rem(sp, 2) == 1, half_swap(line), line)[:, :64]
    act = jnp.concatenate([line, jnp.zeros((6, 64), F32)], axis=0).astype(BF16)
    drain(wmod, lsem.at[1])
    sh = dot(act, wmod[0])
    sc = dot(act, wmod[1])
    ga = dot(act, wmod[2])
    zsend[0:2] = sh[0:2, :128]
    zsend[2:4] = sc[0:2, :128]
    zsend[4:6] = sh[0:2, 128:]
    zsend[6:8] = sc[0:2, 128:]
    zgsend[0:1] = ga[0:1, :128]
    zgsend[1:2] = ga[0:1, 128:]
    zrecv[z] = zsend[...]
    zgrecv[z] = zgsend[...]

    phase("barrier")
    pl.semaphore_wait(barrier, NZ - 1 + NY * NTP - 1)

    phase("z_start")
    def z_copy(k):
        dz = lax.rem(z + k, NZ)
        return remote(zsend, zrecv.at[z], zs, zr, dz * NY + y, tp)

    def zg_copy(k):
        dz = lax.rem(z + k, NZ)
        return remote(zgsend, zgrecv.at[z], zgs, zgr, dz * NY + y, tp)

    far_first = (4, 3, 5, 2, 6, 1, 7)
    for k in far_first:
        z_copy(k).start()
    for k in far_first:
        zg_copy(k).start()

    phase("stats")
    w_copy = remote(wo, wo2, ws, wr, sp, partner)

    drain(lat, lsem.at[2])

    def row_stats(i, c):
        rows = pl.ds(pl.multiple_of(i * 32, 32), 32)
        v = lat[rows, :].astype(F32)
        r = lax.rsqrt(jnp.mean(v * v, axis=1, keepdims=True) + EPSILON)
        rsl[rows, :] = jnp.broadcast_to(r, (32, 128))
        return c

    lax.fori_loop(0, (TOK + CTXL) // 32, row_stats, 0)
    drain(gains, lsem.at[3])
    for t in range(16):
        mod[5:6, 128 * t : 128 * t + 128] = gains[0, t : t + 1, :]
        mod[6:7, 128 * t : 128 * t + 128] = gains[1, t : t + 1, :]
    drain(bias, lsem.at[4])
    biasx[...] = jnp.zeros((16, 128), F32)
    for d in range(2 * WIN_ROWS - 1):
        line = bias[d, pl.ds(y, 1), :]
        biasx[d : d + 1, 0:31] = line
        if d > 0:
            biasx[d - 1 : d, 64:95] = line
    drain(wo, lsem.at[5])

    phase("z_wait")
    drain(zrecv.at[pl.ds(0, NZ - 1)], zr)
    phase("m_start")
    total = zrecv[0]
    for k in range(1, NZ):
        total = total + zrecv[k]
    msend[...] = total
    mrecv[group] = total

    def m_copy(k):
        g = lax.rem(group + k, NY * NTP)
        dy, dt = lax.div(g, NTP), lax.rem(g, NTP)
        return remote(msend, mrecv.at[group], ms, mr, z * NY + dy, dt)

    def m_start(k, c):
        m_copy(k).start()
        return c

    lax.fori_loop(1, NY * NTP, m_start, 0)
    w_copy.start()

    phase("tables")
    col = lax.rem(lax.broadcasted_iota(jnp.int32, (64, 128), 1), 64)
    right = lax.div(lax.broadcasted_iota(jnp.int32, (64, 128), 1), 64)
    qcol = lax.broadcasted_iota(jnp.int32, (64, 128), 0)
    first_col = jnp.clip(qcol - WIN_COLS // 2, 0, GRID_W - WIN_COLS)
    in_cols = (col >= first_col) & (col < first_col + WIN_COLS)
    row0 = z * 16

    def table(t, c):
        p = jnp.where(t < 3, t, t + 3)
        base = jnp.clip(row0 + 2 * p - 4, 0, LAST_START)
        for a in range(2):
            row = row0 + 2 * p + a
            off = jnp.clip(row - 4, 0, LAST_START) - base
            d0 = base - row + 7
            for m in range(5):
                line = biasx[pl.ds(d0 + 2 * m, 1), :]
                tile = pltpu.roll(
                    jnp.broadcast_to(line, (64, 128)), 113, 1, stride=1, stride_axis=0
                )
                krow = right + 2 * m
                ok = in_cols & (krow >= off) & (krow < off + WIN_ROWS)
                btab[t, a * 64 : a * 64 + 64, m * 128 : m * 128 + 128] = jnp.where(
                    ok, tile, -jnp.inf
                )
        return c

    lax.fori_loop(0, len(SPECIAL), table, 0)

    @pl.when(z == 0)
    def _():
        kvext[0:TOK] = jnp.zeros((TOK, 128), BF16)

    @pl.when(z == NZ - 1)
    def _():
        kvext[5 * TOK : 6 * TOK] = jnp.zeros((TOK, 128), BF16)

    phase("m_wait")
    drain(mrecv.at[pl.ds(0, NY * NTP - 1)], mr)
    phase("mod")
    for t in range(NTP):
        total = mrecv[t] + mrecv[NTP + t] + mrecv[2 * NTP + t] + mrecv[3 * NTP + t]
        lo, hi = 256 * t, 256 * t + 128
        mod[0:4, lo : lo + 128] = total[0:4]
        mod[0:4, hi : hi + 128] = total[4:8]
    mod[2:3, :] = mod[5:6, :] * (1.0 + mod[2:3, :])
    mod[3:4, :] = mod[5:6, :] * (1.0 + mod[3:4, :])

    phase("hidden")
    def hidden(rows, which):
        v = lat[rows, :].astype(F32) * rsl[rows, 0:1]
        hid[rows, :] = (v * mod[2 + which : 3 + which, :] + mod[which : 1 + which, :]).astype(BF16)

    def lat_hidden(i, c):
        hidden(pl.ds(pl.multiple_of(i * 32, 32), 32), 0)
        return c

    hidden(pl.ds(TOK, CTXL), 1)
    lax.fori_loop(0, TOK // 32, lat_hidden, 0)
    phase("kv")
    drain(wkv, lsem.at[6])
    kv_all = dot(hid[...], wkv[...])
    kv = kv_all[TOK:]
    for q in range(2):
        kt = kv[:, 128 * q : 128 * q + 128]
        vt = kv[:, 256 + 128 * q : 256 + 128 * q + 128]
        csend[2 * q] = jnp.where(low, kt, half_swap(vt)).astype(BF16)
        csend[2 * q + 1] = jnp.where(low, half_swap(kt), vt).astype(BF16)
    here = pl.ds(pl.multiple_of(sp * CTXL, CTXL), CTXL)
    ctxkv[here, :] = csend[y]

    def c_copy(k):
        d = lax.rem(sp + k, NZ * NY)
        return remote(csend.at[lax.rem(d, NY)], ctxkv.at[here, :], cs, cr, d, tp)

    def c_start(k, c):
        c_copy(k).start()
        return c

    lax.fori_loop(1, NZ * NY, c_start, 0)

    kv = kv_all[:TOK]
    for q in range(2):
        kt = kv[:, 128 * q : 128 * q + 128]
        vt = kv[:, 256 + 128 * q : 256 + 128 * q + 128]
        kvsend[2 * q] = jnp.where(low, kt, half_swap(vt)).astype(BF16)
        kvsend[2 * q + 1] = jnp.where(low, half_swap(kt), vt).astype(BF16)
    mine = pl.ds(pl.multiple_of((1 + y) * TOK, TOK), TOK)
    kvext[mine, :] = kvsend[y]

    def k_copy(k):
        dy = lax.rem(y + k, NY)
        return remote(kvsend.at[dy], kvext.at[mine, :], ks, kr.at[y], z * NY + dy, tp)

    def k_in(dy):
        rows = pl.ds(pl.multiple_of((1 + dy) * TOK, TOK), TOK)
        return remote(kvsend.at[y], kvext.at[rows, :], ks, kr.at[dy], z * NY + dy, tp)

    for k in (2, 1, 3):
        k_copy(k).start()

    phase("qg")
    drain(wqg, lsem.at[7])
    qg = dot(hid[0:TOK, :], wqg[:, 0:TOK])
    for q in range(2):
        qt = qg[:, 128 * q : 128 * q + 128] * (HD**-0.5)
        up, dn = qt[0:128], qt[128:256]
        qsend[2 * q] = jnp.where(low, up, half_swap(dn)).astype(BF16)
        qsend[2 * q + 1] = jnp.where(low, half_swap(up), dn).astype(BF16)
    qrecv[y] = qsend[y]

    def q_copy(k):
        dy = lax.rem(y + k, NY)
        return remote(qsend.at[dy], qrecv.at[y], qs, qr, z * NY + dy, tp)

    for k in (2, 1, 3):
        q_copy(k).start()
    phase("g")
    g = dot(hid[0:TOK, :], wqg[:, TOK:])
    gbuf[...] = g.astype(BF16).reshape(NX, NC, OUTR, TOK)
    g_copy = remote(gbuf.at[:, 1 - core], gother, gs, gr, sp, partner)
    g_copy.start()

    phase("kq_wait")
    drain(zgrecv.at[pl.ds(0, NZ - 1)], zgr)
    total = zgrecv[0]
    for k in range(1, NZ):
        total = total + zgrecv[k]
    mgsend[...] = total
    mgrecv[group] = total

    def mg_copy(k):
        g = lax.rem(group + k, NY * NTP)
        dy, dt = lax.div(g, NTP), lax.rem(g, NTP)
        return remote(mgsend, mgrecv.at[group], mgs, mgr, z * NY + dy, dt)

    def mg_start(k, c):
        mg_copy(k).start()
        return c

    lax.fori_loop(1, NY * NTP, mg_start, 0)

    up_src = kvext.at[pl.ds(4 * TOK, TOK), :]
    dn_src = kvext.at[pl.ds(TOK, TOK), :]
    up_dst = kvext.at[pl.ds(0, TOK), :]
    dn_dst = kvext.at[pl.ds(5 * TOK, TOK), :]
    up_copy = remote(up_src, up_dst, hs.at[0], hr.at[0], jnp.minimum(z + 1, NZ - 1) * NY + y, tp)
    dn_copy = remote(dn_src, dn_dst, hs.at[1], hr.at[1], jnp.maximum(z - 1, 0) * NY + y, tp)

    @pl.when(y != 3)
    def _():
        k_in(3).wait_recv()

    @pl.when(z < NZ - 1)
    def _():
        up_copy.start()

    @pl.when(y != 0)
    def _():
        k_in(0).wait_recv()

    @pl.when(z > 0)
    def _():
        dn_copy.start()

    @pl.when(y != 1)
    def _():
        k_in(1).wait_recv()

    @pl.when(y != 2)
    def _():
        k_in(2).wait_recv()

    phase("gates")
    g_copy.wait_recv()
    for part in range(2):
        g = (gbuf[:, core] if part == 0 else gother[...]).astype(F32)
        sgate[:, :, TOK * part : TOK * part + TOK] = g * (1.0 / (1.0 + jnp.exp(-g)))
    phase("q_wait")
    drain(qrecv.at[pl.ds(0, NY - 1)], qr)
    phase("c_wait")
    drain(ctxkv.at[pl.ds(0, CTX - CTXL)], cr)
    phase("h_wait")
    @pl.when(z > 0)
    def _():
        up_copy.wait_recv()

    @pl.when(z < NZ - 1)
    def _():
        dn_copy.wait_recv()

    phase("attention")
    first = 1 - lax.div(x, 2)
    beside = x + 1 - 2 * lax.rem(x, 2)
    source = core * NY + y

    def r_copy(a, b, h):
        return remote(
            rsend.at[a, b, h], rrecv.at[a, source], rs, rr.at[a], z * NY + b, x * NC + h
        )

    def pair(a, k):
        b = lax.rem(y + k, NY)
        p = 2 * b + a
        xq = qrecv[b].astype(F32)
        qp = jnp.where(low, jnp.where(a == 1, half_swap(xq), xq), 0.0).astype(BF16)
        base = jnp.clip(row0 + 2 * p - 4, 0, LAST_START) - row0 + 4
        rows = pl.ds(pl.multiple_of(base * GRID_W, GRID_W), 10 * GRID_W)
        t = jnp.where(p < 2, p, jnp.where(p < 6, 2, p - 3))
        sc_ctx = dot_nt(qp, ctxkv[...])
        kvw = kvext[rows, :]
        sc_win = dot_nt(qp, kvw) + btab[t]
        top = jnp.maximum(
            jnp.max(sc_ctx, axis=1, keepdims=True), jnp.max(sc_win, axis=1, keepdims=True)
        )
        e_ctx = jnp.exp(sc_ctx - top)
        e_win = jnp.exp(sc_win - top)
        den = jnp.sum(e_ctx, axis=1, keepdims=True) + jnp.sum(e_win, axis=1, keepdims=True)
        o = dot(e_ctx.astype(BF16), ctxkv[...]) + dot(e_win.astype(BF16), kvw)
        o = o * (1.0 / den)
        for h in range(NC):
            r0, r1 = o[OUTR * h : OUTR * h + OUTR], o[64 + OUTR * h : 64 + OUTR * h + OUTR]
            rsend[a, b, h] = jnp.where(low, half_swap(r0), r1).astype(BF16)

    def send_back(a, k):
        b = lax.rem(y + k, NY)
        for h in range(NC):
            r_copy(a, b, h).start()

    def far_pairs(a):
        pair(a, 1)
        pair(a, 2)
        send_back(a, 1)
        send_back(a, 2)

    def near_pairs(a):
        pair(a, 3)
        pair(a, 0)
        send_back(a, 3)
        r_copy(a, y, 1 - core).start()
        rrecv[a, source] = rsend[a, y, core]

    def p_copy(i):
        return remote(psend.at[i], precv.at[x], ps, pr, sp, i * NC + core)

    def finish(a):
        phase("r_wait")
        drain(rrecv.at[a, pl.ds(0, NC * NY - 1)], rr.at[a])
        phase("project")
        for part in range(2):
            src = (core if part == 0 else 1 - core) * NY
            for q in range(2):
                x0, x1 = rrecv[a, src + 2 * q].astype(F32), rrecv[a, src + 2 * q + 1].astype(F32)
                cols = slice(TOK * part + 128 * q, TOK * part + 128 * q + 128)
                up = jnp.where(low, x0, half_swap(x1)) * sgate[2 * a, :, cols]
                dn = jnp.where(low, half_swap(x0), x1) * sgate[2 * a + 1, :, cols]
                gated[0:OUTR, cols] = up.astype(BF16)
                gated[OUTR : 2 * OUTR, cols] = dn.astype(BF16)
        for n in range(4):
            cols = slice(512 * n, 512 * n + 512)
            term = dot(gated[:, :TOK], wo[:, cols]) + dot(gated[:, TOK:], wo2[:, cols])
            psend[2 * a, :, cols] = term[:OUTR].astype(BF16)
            psend[2 * a + 1, :, cols] = term[OUTR:].astype(BF16)

    far_pairs(first)
    near_pairs(first)
    phase("attention2")
    far_pairs(1 - first)
    near_pairs(1 - first)
    phase("w_wait")
    w_copy.wait_recv()
    finish(first)
    p_copy(lax.rem(x + 2, NX)).start()
    p_copy(lax.rem(beside + 2, NX)).start()
    finish(1 - first)
    p_copy(beside).start()

    phase("sent1")
    drain(zrecv.at[pl.ds(0, NZ - 1)], zs)
    drain(zgrecv.at[pl.ds(0, NZ - 1)], zgs)
    drain(mrecv.at[pl.ds(0, NY * NTP - 1)], ms)
    drain(mgrecv.at[pl.ds(0, NY * NTP - 1)], mgs)
    drain(mgrecv.at[pl.ds(0, NY * NTP - 1)], mgr)
    drain(ctxkv.at[pl.ds(0, CTX - CTXL)], cs)
    drain(kvext.at[pl.ds(0, (NY - 1) * TOK)], ks)
    drain(qrecv.at[pl.ds(0, NY - 1)], qs)
    w_copy.wait_send()
    g_copy.wait_send()
    for a in range(2):
        drain(rrecv.at[a, pl.ds(0, NC * NY - 1)], rs)

    @pl.when(z < NZ - 1)
    def _():
        up_copy.wait_send()

    @pl.when(z > 0)
    def _():
        dn_copy.wait_send()

    for t in range(NTP):
        total = mgrecv[t] + mgrecv[NTP + t] + mgrecv[2 * NTP + t] + mgrecv[3 * NTP + t]
        mod[4:5, 256 * t : 256 * t + 128] = total[0:1]
        mod[4:5, 256 * t + 128 : 256 * t + 256] = total[1:2]
    phase("p_wait")
    drain(precv.at[pl.ds(0, NX - 1)], pr)
    phase("final")
    branch = psend[x].astype(F32)
    for k in (1, 2, 3):
        branch = branch + precv[lax.rem(x + k, NX)].astype(F32)
    branch = branch.astype(BF16).astype(F32)
    normed = branch * lax.rsqrt(jnp.mean(branch * branch, axis=1, keepdims=True) + EPSILON)
    own = lat[pl.ds(pl.multiple_of(tp * OUTR, OUTR), OUTR), :].astype(F32)
    out_ref[...] = (own + mod[4:5, :] * (normed * mod[6:7, :])).astype(BF16)

    phase("sent")
    drain(precv.at[pl.ds(0, NX - 1)], ps)
    phase(None)


def shards(
    latent,
    context,
    condition,
    context_condition,
    gain_pre,
    gain_post,
    w_shift,
    w_scale,
    w_gate,
    w_query,
    w_key,
    w_value,
    w_silu,
    offset_bias,
    w_out,
):
    in_rows = w_shift.shape[0]
    vmem = pl.BlockSpec(memory_space=pltpu.VMEM)
    hbm = pl.BlockSpec(memory_space=pltpu.HBM)
    dma = pltpu.SemaphoreType.DMA
    operands = (
        condition.reshape(16, 128),
        context_condition.reshape(16, 128),
        gain_pre.reshape(16, 128),
        gain_post.reshape(16, 128),
        jnp.transpose(offset_bias, (1, 0, 2)),
        latent,
        context,
        w_shift,
        w_scale,
        w_gate,
        w_query,
        w_key,
        w_value,
        w_silu,
        w_out,
    )
    operands = [pltpu.with_memory_space_constraint(a, pltpu.HBM) for a in operands]
    return pl.pallas_call(
        kernel,
        name="whole",
        out_shape=jax.ShapeDtypeStruct((OUTR, D), BF16),
        in_specs=[hbm] * 15,
        out_specs=vmem,
        scratch_shapes=[
            pltpu.VMEM((2, 16, 128), BF16),
            pltpu.VMEM((2, 16, 128), F32),
            pltpu.VMEM((2, 16, 128), F32),
            pltpu.VMEM((2 * WIN_ROWS - 1, NY, 2 * WIN_COLS - 1), F32),
            pltpu.VMEM((16, 128), F32),
            pltpu.VMEM((3, in_rows, TOK), BF16),
            pltpu.VMEM((TOK + CTXL, D), BF16),
            pltpu.VMEM((D, 2 * TOK), BF16),
            pltpu.VMEM((D, 2 * TOK), BF16),
            pltpu.VMEM((TOK, D), BF16),
            pltpu.VMEM((TOK, D), BF16),
            pltpu.VMEM((8, 128), F32),
            pltpu.VMEM((NZ, 8, 128), F32),
            pltpu.VMEM((8, 128), F32),
            pltpu.VMEM((NY * NTP, 8, 128), F32),
            pltpu.VMEM((2, 128), F32),
            pltpu.VMEM((NZ, 2, 128), F32),
            pltpu.VMEM((2, 128), F32),
            pltpu.VMEM((NY * NTP, 2, 128), F32),
            pltpu.VMEM((8, D), F32),
            pltpu.VMEM((len(SPECIAL), 128, 640), F32),
            pltpu.VMEM((TOK + CTXL, D), BF16),
            pltpu.VMEM((TOK + CTXL, 128), F32),
            pltpu.VMEM((NY, CTXL, 128), BF16),
            pltpu.VMEM((CTX, 128), BF16),
            pltpu.VMEM((NY, TOK, 128), BF16),
            pltpu.VMEM((6 * TOK, 128), BF16),
            pltpu.VMEM((NY, 128, 128), BF16),
            pltpu.VMEM((NY, 128, 128), BF16),
            pltpu.VMEM((NX, NC, OUTR, TOK), BF16),
            pltpu.VMEM((NX, OUTR, TOK), BF16),
            pltpu.VMEM((NX, OUTR, NC * TOK), F32),
            pltpu.VMEM((2, NY, NC, OUTR, 128), BF16),
            pltpu.VMEM((2, NC * NY, OUTR, 128), BF16),
            pltpu.VMEM((2 * OUTR, NC * TOK), BF16),
            pltpu.VMEM((NX, OUTR, D), BF16),
            pltpu.VMEM((NX, OUTR, D), BF16),
            dma((8,)),
            dma,
            dma,
            dma,
            dma,
            dma,
            dma,
            dma,
            dma,
            dma,
            dma,
            dma,
            dma,
            dma,
            dma((NY,)),
            dma,
            dma,
            dma((2,)),
            dma((2,)),
            dma,
            dma((2,)),
            dma,
            dma,
            dma,
            dma,
        ],
        compiler_params=pltpu.CompilerParams(
            collective_id=0, has_side_effects=True, vmem_limit_bytes=48 << 20
        ),
    )(*operands)


def solution(mesh):
    in_specs = (
        P("sp", None),
        P("sp", None),
        P(),
        P(),
        P(),
        P(),
        P("sp", "tp"),
        P("sp", "tp"),
        P("sp", "tp"),
        P(None, "tp"),
        P(None, "tp"),
        P(None, "tp"),
        P(None, "tp"),
        P("tp", None, None),
        P("tp", None),
    )
    out_specs = P(("sp", "tp"), None)
    return jax.shard_map(shards, mesh=mesh, in_specs=in_specs, out_specs=out_specs, check_vma=False)
```

time: 55 us -> 49.5 us (0.900)
  Pallas kernels: 53.3 us -> 48.7 us
  local copies, waits for them, and re-layouts: 1.57 us -> 0.66 us
    pallas_call x1, Pallas kernels: 53.3 us -> 48.7 us  [shards(): pl.pallas_call(kernel, name='whole', out_shape=jax.ShapeDtypeStruct((OUTR...]
    unnamed x1, local copies, waits for them, and re-layouts: 1.57 us -> 0.66 us
where the time goes in v3:
time: 49.5 us; the launch traced here: 49.4 us
  Pallas kernels  48.7 us (98%)
  local copies, waits for them, and re-layouts  0.66 us (1%)
    pallas_call x1, Pallas kernels, shards(): pl.pallas_call(kernel, name='whole', out_shape=jax.ShapeDtypeStruct((OUTR...  48.7 us

profile of v3, /device:TPU:1, one launch (start us, length us, event | category | flops | bytes accessed | tf_op | source)
XLA Modules:
  0.0 49.4 jit_solution(16375205700386116953)
XLA Ops:
  0.0 48.7 %whole.1 = bf16[32,2048]{1,0:T(8,128)(2,1)S(1)} custom-call(bf16[16,128]{1,0:T(8,128)(2,1)} %bitcast.8, bf16[16,128]{1,0:T(8,128)(2,1)} %bitcast.9, f32[16,128]{1,0:T(8,128)} %bitcast.6, f32[16,128]{1,0:T(8,128)} %bitcast.7, f32[15,4,31]{2,1,0:T(4,128)} %bitcast.5, bf16[256,2048]{1,0:T(8,128)(2,1)} %lat_h.1, bf16[32,2048]{1,0:T(8,128)(2,1)} %ctx_h.1, ...), custom_call_target="tpu_custom_call" | custom-call | tf_op jit(solution)/shard_map/whole/pallas_call | solution.py:636
  48.7 0.7 %copy.17 = bf16[32,2048]{1,0:T(8,128)(2,1)} copy(bf16[32,2048]{1,0:T(8,128)(2,1)S(1)} %whole.1) | data formatting | bytes 262144

commit v4 on v3

--- a/solution.py
+++ b/solution.py
@@ -90,7 +90,9 @@
     biasx,
     wmod,
     lat,
+    ctx,
     wkv,
+    wy,
     wqg,
     wo,
     wo2,
@@ -103,10 +105,12 @@
     mgsend,
     mgrecv,
     mod,
+    spread,
     btab,
     hid,
+    hidc,
     rsl,
-    csend,
+    rsc,
     ctxkv,
     kvsend,
     kvext,
@@ -129,6 +133,10 @@
     zgr,
     mgs,
     mgr,
+    xs,
+    xr,
+    xps,
+    xpr,
     ws,
     wr,
     cs,
@@ -163,7 +171,9 @@
 
     load(0, (cond_h, conds.at[0]), (cond2_h, conds.at[1]))
     load(1, (wsh_h, wmod.at[0]), (wsc_h, wmod.at[1]), (wga_h, wmod.at[2]))
-    load(2, (ctx_h, lat.at[pl.ds(TOK, CTXL), :]), (lat_h, lat.at[pl.ds(0, TOK), :]))
+    half = CTXL // NC
+    load(8, *((ctx_h.at[pl.ds(half * h, half), :], ctx.at[y, h]) for h in range(NC)))
+    load(2, (lat_h, lat))
     load(3, (gpre_h, gains.at[0]), (gpost_h, gains.at[1]))
     load(4, (bias_h, bias))
     load(5, (wo_h, wo))
@@ -228,19 +238,31 @@
     for k in far_first:
         zg_copy(k).start()
 
+    def x_copy(k):
+        dy = lax.rem(y + k, NY)
+        return remote(ctx.at[y, core], ctx.at[y, core], xs, xr, z * NY + dy, tp)
+
+    def x_pass(k):
+        rows = ctx.at[lax.rem(y + k, NY), core]
+        return remote(rows, rows, xps, xpr, sp, partner)
+
+    drain(ctx.at[0], lsem.at[8])
+    for k in (2, 1, 3):
+        x_copy(k).start()
+
     phase("stats")
-    w_copy = remote(wo, wo2, ws, wr, sp, partner)
-
     drain(lat, lsem.at[2])
+
+    def stats(v):
+        r = lax.rsqrt(jnp.mean(v * v, axis=1, keepdims=True) + EPSILON)
+        return jnp.broadcast_to(r, (v.shape[0], 128))
 
     def row_stats(i, c):
         rows = pl.ds(pl.multiple_of(i * 32, 32), 32)
-        v = lat[rows, :].astype(F32)
-        r = lax.rsqrt(jnp.mean(v * v, axis=1, keepdims=True) + EPSILON)
-        rsl[rows, :] = jnp.broadcast_to(r, (32, 128))
+        rsl[rows, :] = stats(lat[rows, :].astype(F32))
         return c
 
-    lax.fori_loop(0, (TOK + CTXL) // 32, row_stats, 0)
+    lax.fori_loop(0, TOK // 32, row_stats, 0)
     drain(gains, lsem.at[3])
     for t in range(16):
         mod[5:6, 128 * t : 128 * t + 128] = gains[0, t : t + 1, :]
@@ -252,7 +274,6 @@
         biasx[d : d + 1, 0:31] = line
         if d > 0:
             biasx[d - 1 : d, 64:95] = line
-    drain(wo, lsem.at[5])
 
     phase("z_wait")
     drain(zrecv.at[pl.ds(0, NZ - 1)], zr)
@@ -273,7 +294,6 @@
         return c
 
     lax.fori_loop(1, NY * NTP, m_start, 0)
-    w_copy.start()
 
     phase("tables")
     col = lax.rem(lax.broadcasted_iota(jnp.int32, (64, 128), 1), 64)
@@ -312,6 +332,32 @@
     def _():
         kvext[5 * TOK : 6 * TOK] = jnp.zeros((TOK, 128), BF16)
 
+    phase("x_wait")
+    drain(ctx.at[pl.ds(0, NY - 1), 0], xr)
+    for k in (1, 2, 3):
+        x_pass(k).start()
+
+    phase("wy")
+    drain(wkv, lsem.at[6])
+
+    def head_columns(i, c):
+        rows = pl.ds(pl.multiple_of(i * 256, 256), 256)
+        at = 128 * lax.div(y, 2)
+        kt = wkv[rows, pl.ds(pl.multiple_of(at, 128), 128)].astype(F32)
+        vt = wkv[rows, pl.ds(pl.multiple_of(TOK + at, 128), 128)].astype(F32)
+        odd = lax.rem(y, 2) == 1
+        wy[rows, :] = jnp.where(
+            low, jnp.where(odd, half_swap(kt), kt), jnp.where(odd, vt, half_swap(vt))
+        ).astype(BF16)
+        return c
+
+    lax.fori_loop(0, D // 256, head_columns, 0)
+    phase("x_wait2")
+    drain(ctx.at[pl.ds(0, NY - 1), 0], xpr)
+    for b in range(NY):
+        rows = slice(CTXL * b, CTXL * b + CTXL)
+        rsc[rows, :] = stats(ctx[b].reshape(CTXL, D).astype(F32))
+
     phase("m_wait")
     drain(mrecv.at[pl.ds(0, NY * NTP - 1)], mr)
     phase("mod")
@@ -323,45 +369,47 @@
     mod[2:3, :] = mod[5:6, :] * (1.0 + mod[2:3, :])
     mod[3:4, :] = mod[5:6, :] * (1.0 + mod[3:4, :])
 
-    phase("hidden")
-    def hidden(rows, which):
-        v = lat[rows, :].astype(F32) * rsl[rows, 0:1]
-        hid[rows, :] = (v * mod[2 + which : 3 + which, :] + mod[which : 1 + which, :]).astype(BF16)
-
-    def lat_hidden(i, c):
-        hidden(pl.ds(pl.multiple_of(i * 32, 32), 32), 0)
-        return c
-
-    hidden(pl.ds(TOK, CTXL), 1)
-    lax.fori_loop(0, TOK // 32, lat_hidden, 0)
-    phase("kv")
-    drain(wkv, lsem.at[6])
-    kv_all = dot(hid[...], wkv[...])
-    kv = kv_all[TOK:]
-    for q in range(2):
-        kt = kv[:, 128 * q : 128 * q + 128]
-        vt = kv[:, 256 + 128 * q : 256 + 128 * q + 128]
-        csend[2 * q] = jnp.where(low, kt, half_swap(vt)).astype(BF16)
-        csend[2 * q + 1] = jnp.where(low, half_swap(kt), vt).astype(BF16)
-    here = pl.ds(pl.multiple_of(sp * CTXL, CTXL), CTXL)
-    ctxkv[here, :] = csend[y]
+    for i in range(4):
+        spread[i] = jnp.broadcast_to(mod[i : i + 1, :], (8, D))
+
+    def hidden(v, r, which):
+        n = v.shape[0] // 8
+        r = r.reshape(n, 8, 128)
+        parts = []
+        for t in range(D // 128):
+            cols = slice(128 * t, 128 * t + 128)
+            u = v[:, cols].astype(F32).reshape(n, 8, 128) * r
+            u = u * spread[2 + which, :, cols] + spread[which, :, cols]
+            parts.append(u.reshape(8 * n, 128).astype(BF16))
+        return jnp.concatenate(parts, axis=1)
+
+    phase("ctx_hidden")
+    for b in range(NY):
+        rows = slice(CTXL * b, CTXL * b + CTXL)
+        hidc[rows, :] = hidden(ctx[b].reshape(CTXL, D), rsc[rows, :], 1)
+    phase("ctx_kv")
+    here = pl.ds(pl.multiple_of(z * NY * CTXL, NY * CTXL), NY * CTXL)
+    ctxkv[here, :] = dot(hidc[...], wy[...]).astype(BF16)
 
     def c_copy(k):
-        d = lax.rem(sp + k, NZ * NY)
-        return remote(csend.at[lax.rem(d, NY)], ctxkv.at[here, :], cs, cr, d, tp)
-
-    def c_start(k, c):
+        dz = lax.rem(z + k, NZ)
+        return remote(ctxkv.at[here, :], ctxkv.at[here, :], cs, cr, dz * NY + y, tp)
+
+    for k in far_first:
         c_copy(k).start()
-        return c
-
-    lax.fori_loop(1, NZ * NY, c_start, 0)
-
-    kv = kv_all[:TOK]
-    for q in range(2):
-        kt = kv[:, 128 * q : 128 * q + 128]
-        vt = kv[:, 256 + 128 * q : 256 + 128 * q + 128]
-        kvsend[2 * q] = jnp.where(low, kt, half_swap(vt)).astype(BF16)
-        kvsend[2 * q + 1] = jnp.where(low, half_swap(kt), vt).astype(BF16)
+
+    phase("hidden_kv")
+    for i in range(2):
+        rows = slice(128 * i, 128 * i + 128)
+        for n in range(4):
+            r32 = slice(128 * i + 32 * n, 128 * i + 32 * n + 32)
+            hid[r32, :] = hidden(lat[r32, :], rsl[r32, :], 0)
+        kv = dot(hid[rows, :], wkv[...])
+        for q in range(2):
+            kt = kv[:, 128 * q : 128 * q + 128]
+            vt = kv[:, 256 + 128 * q : 256 + 128 * q + 128]
+            kvsend[2 * q, rows] = jnp.where(low, kt, half_swap(vt)).astype(BF16)
+            kvsend[2 * q + 1, rows] = jnp.where(low, half_swap(kt), vt).astype(BF16)
     mine = pl.ds(pl.multiple_of((1 + y) * TOK, TOK), TOK)
     kvext[mine, :] = kvsend[y]
 
@@ -397,6 +445,9 @@
     gbuf[...] = g.astype(BF16).reshape(NX, NC, OUTR, TOK)
     g_copy = remote(gbuf.at[:, 1 - core], gother, gs, gr, sp, partner)
     g_copy.start()
+    drain(wo, lsem.at[5])
+    w_copy = remote(wo, wo2, ws, wr, sp, partner)
+    w_copy.start()
 
     phase("kq_wait")
     drain(zgrecv.at[pl.ds(0, NZ - 1)], zgr)
@@ -456,17 +507,7 @@
     phase("q_wait")
     drain(qrecv.at[pl.ds(0, NY - 1)], qr)
     phase("c_wait")
-    drain(ctxkv.at[pl.ds(0, CTX - CTXL)], cr)
-    phase("h_wait")
-    @pl.when(z > 0)
-    def _():
-        up_copy.wait_recv()
-
-    @pl.when(z < NZ - 1)
-    def _():
-        dn_copy.wait_recv()
-
-    phase("attention")
+    drain(ctxkv.at[pl.ds(0, CTX - NY * CTXL)], cr)
     first = 1 - lax.div(x, 2)
     beside = x + 1 - 2 * lax.rem(x, 2)
     source = core * NY + y
@@ -476,8 +517,7 @@
             rsend.at[a, b, h], rrecv.at[a, source], rs, rr.at[a], z * NY + b, x * NC + h
         )
 
-    def pair(a, k):
-        b = lax.rem(y + k, NY)
+    def pair(a, b):
         p = 2 * b + a
         xq = qrecv[b].astype(F32)
         qp = jnp.where(low, jnp.where(a == 1, half_swap(xq), xq), 0.0).astype(BF16)
@@ -499,23 +539,20 @@
             r0, r1 = o[OUTR * h : OUTR * h + OUTR], o[64 + OUTR * h : 64 + OUTR * h + OUTR]
             rsend[a, b, h] = jnp.where(low, half_swap(r0), r1).astype(BF16)
 
-    def send_back(a, k):
-        b = lax.rem(y + k, NY)
-        for h in range(NC):
-            r_copy(a, b, h).start()
-
-    def far_pairs(a):
-        pair(a, 1)
-        pair(a, 2)
-        send_back(a, 1)
-        send_back(a, 2)
-
-    def near_pairs(a):
-        pair(a, 3)
-        pair(a, 0)
-        send_back(a, 3)
-        r_copy(a, y, 1 - core).start()
-        rrecv[a, source] = rsend[a, y, core]
+    def pairs(a, *blocks):
+        for b in blocks:
+            pair(a, b)
+        for b in blocks:
+            for h in range(NC):
+                here = (b == y) & (h == core)
+
+                @pl.when(here)
+                def _():
+                    rrecv[a, source] = rsend[a, b, h]
+
+                @pl.when(jnp.logical_not(here))
+                def _():
+                    r_copy(a, b, h).start()
 
     def p_copy(i):
         return remote(psend.at[i], precv.at[x], ps, pr, sp, i * NC + core)
@@ -539,11 +576,22 @@
             psend[2 * a, :, cols] = term[:OUTR].astype(BF16)
             psend[2 * a + 1, :, cols] = term[OUTR:].astype(BF16)
 
-    far_pairs(first)
-    near_pairs(first)
+    pairs(first, 1, 2)
+    phase("h_wait")
+
+    @pl.when(z > 0)
+    def _():
+        up_copy.wait_recv()
+
+    @pl.when(z < NZ - 1)
+    def _():
+        dn_copy.wait_recv()
+
     phase("attention2")
-    far_pairs(1 - first)
-    near_pairs(1 - first)
+    pairs(first, 0, 3)
+    phase("attention3")
+    pairs(1 - first, 1, 2)
+    pairs(1 - first, 0, 3)
     phase("w_wait")
     w_copy.wait_recv()
     finish(first)
@@ -558,7 +606,9 @@
     drain(mrecv.at[pl.ds(0, NY * NTP - 1)], ms)
     drain(mgrecv.at[pl.ds(0, NY * NTP - 1)], mgs)
     drain(mgrecv.at[pl.ds(0, NY * NTP - 1)], mgr)
-    drain(ctxkv.at[pl.ds(0, CTX - CTXL)], cs)
+    drain(ctxkv.at[pl.ds(0, CTX - NY * CTXL)], cs)
+    drain(ctx.at[pl.ds(0, NY - 1), 0], xs)
+    drain(ctx.at[pl.ds(0, NY - 1), 0], xps)
     drain(kvext.at[pl.ds(0, (NY - 1) * TOK)], ks)
     drain(qrecv.at[pl.ds(0, NY - 1)], qs)
     w_copy.wait_send()
@@ -646,8 +696,10 @@
             pltpu.VMEM((2 * WIN_ROWS - 1, NY, 2 * WIN_COLS - 1), F32),
             pltpu.VMEM((16, 128), F32),
             pltpu.VMEM((3, in_rows, TOK), BF16),
-            pltpu.VMEM((TOK + CTXL, D), BF16),
+            pltpu.VMEM((TOK, D), BF16),
+            pltpu.VMEM((NY, NC, CTXL // NC, D), BF16),
             pltpu.VMEM((D, 2 * TOK), BF16),
+            pltpu.VMEM((D, 128), BF16),
             pltpu.VMEM((D, 2 * TOK), BF16),
             pltpu.VMEM((TOK, D), BF16),
             pltpu.VMEM((TOK, D), BF16),
@@ -660,10 +712,12 @@
             pltpu.VMEM((2, 128), F32),
             pltpu.VMEM((NY * NTP, 2, 128), F32),
             pltpu.VMEM((8, D), F32),
+            pltpu.VMEM((4, 8, D), F32),
             pltpu.VMEM((len(SPECIAL), 128, 640), F32),
-            pltpu.VMEM((TOK + CTXL, D), BF16),
-            pltpu.VMEM((TOK + CTXL, 128), F32),
-            pltpu.VMEM((NY, CTXL, 128), BF16),
+            pltpu.VMEM((TOK, D), BF16),
+            pltpu.VMEM((NY * CTXL, D), BF16),
+            pltpu.VMEM((TOK, 128), F32),
+            pltpu.VMEM((NY * CTXL, 128), F32),
             pltpu.VMEM((CTX, 128), BF16),
             pltpu.VMEM((NY, TOK, 128), BF16),
             pltpu.VMEM((6 * TOK, 128), BF16),
@@ -677,7 +731,11 @@
             pltpu.VMEM((2 * OUTR, NC * TOK), BF16),
             pltpu.VMEM((NX, OUTR, D), BF16),
             pltpu.VMEM((NX, OUTR, D), BF16),
-            dma((8,)),
+            dma((9,)),
+            dma,
+            dma,
+            dma,
+            dma,
             dma,
             dma,
             dma,

time: 49.5 us -> 45.7 us (0.923)
  Pallas kernels: 48.7 us -> 44.9 us
    pallas_call x1, Pallas kernels: 48.7 us -> 44.9 us  [shards(): pl.pallas_call(kernel, name='whole', out_shape=jax.ShapeDtypeStruct((OUTR...]
where the time goes in v4:
time: 45.7 us; the launch traced here: 45.6 us
  Pallas kernels  44.9 us (98%)
  local copies, waits for them, and re-layouts  0.66 us (1%)
    pallas_call x1, Pallas kernels, shards(): pl.pallas_call(kernel, name='whole', out_shape=jax.ShapeDtypeStruct((OUTR...  44.9 us

profile of v4, /device:TPU:1, one launch (start us, length us, event | category | flops | bytes accessed | tf_op | source)
XLA Modules:
  0.0 45.6 jit_solution(564178606616258788)
XLA Ops:
  0.0 44.9 %whole.1 = bf16[32,2048]{1,0:T(8,128)(2,1)S(1)} custom-call(bf16[16,128]{1,0:T(8,128)(2,1)} %bitcast.8, bf16[16,128]{1,0:T(8,128)(2,1)} %bitcast.9, f32[16,128]{1,0:T(8,128)} %bitcast.6, f32[16,128]{1,0:T(8,128)} %bitcast.7, f32[15,4,31]{2,1,0:T(4,128)} %bitcast.5, bf16[256,2048]{1,0:T(8,128)(2,1)} %lat_h.1, bf16[32,2048]{1,0:T(8,128)(2,1)} %ctx_h.1, ...), custom_call_target="tpu_custom_call" | custom-call | tf_op jit(solution)/shard_map/whole/pallas_call | solution.py:686
  44.9 0.7 %copy.17 = bf16[32,2048]{1,0:T(8,128)(2,1)} copy(bf16[32,2048]{1,0:T(8,128)(2,1)S(1)} %whole.1) | data formatting | bytes 262144

commit v5 on v4

--- a/solution.py
+++ b/solution.py
@@ -21,6 +21,11 @@
 OUTR = TOK // NTP
 LAST_START = NZ * NY * TOK // GRID_W - WIN_ROWS
 SPECIAL = (0, 1, 2, 6, 7)
+Z_ORDER = (4, 3, 5, 2, 6, 1, 7)
+G_ORDER = sorted(
+    ((ky, kx, kc) for ky in range(NY) for kx in range(NX) for kc in range(NC)),
+    key=lambda k: -min(k[0], NY - k[0]) - min(k[1], NX - k[1]) - k[2] / 2,
+)[:-1]
 F32 = jnp.float32
 BF16 = jnp.bfloat16
 NT = (((1,), (1,)), ((), ()))
@@ -188,17 +193,15 @@
             barrier, inc=1, device_id=(dsp, dtp), device_id_type=pl.DeviceIdType.MESH
         )
 
-    def greet_z(k, c):
+    for k in Z_ORDER:
         greet(lax.rem(z + k, NZ) * NY + y, tp)
-        return c
-
-    def greet_g(k, c):
-        g = lax.rem(group + k, NY * NTP)
-        greet(z * NY + lax.div(g, NTP), lax.rem(g, NTP))
-        return c
-
-    lax.fori_loop(1, NZ, greet_z, 0)
-    lax.fori_loop(1, NY * NTP, greet_g, 0)
+
+    def group_peer(k):
+        dx, dc = lax.rem(x + k[1], NX), 1 - core if k[2] else core
+        return z * NY + lax.rem(y + k[0], NY), dx * NC + dc
+
+    for k in G_ORDER:
+        greet(*group_peer(k))
 
     phase("partial")
     drain(conds, lsem.at[0])
@@ -232,10 +235,9 @@
         dz = lax.rem(z + k, NZ)
         return remote(zgsend, zgrecv.at[z], zgs, zgr, dz * NY + y, tp)
 
-    far_first = (4, 3, 5, 2, 6, 1, 7)
-    for k in far_first:
+    for k in Z_ORDER:
         z_copy(k).start()
-    for k in far_first:
+    for k in Z_ORDER:
         zg_copy(k).start()
 
     def x_copy(k):
@@ -284,16 +286,8 @@
     msend[...] = total
     mrecv[group] = total
 
-    def m_copy(k):
-        g = lax.rem(group + k, NY * NTP)
-        dy, dt = lax.div(g, NTP), lax.rem(g, NTP)
-        return remote(msend, mrecv.at[group], ms, mr, z * NY + dy, dt)
-
-    def m_start(k, c):
-        m_copy(k).start()
-        return c
-
-    lax.fori_loop(1, NY * NTP, m_start, 0)
+    for k in G_ORDER:
+        remote(msend, mrecv.at[group], ms, mr, *group_peer(k)).start()
 
     phase("tables")
     col = lax.rem(lax.broadcasted_iota(jnp.int32, (64, 128), 1), 64)
@@ -395,7 +389,7 @@
         dz = lax.rem(z + k, NZ)
         return remote(ctxkv.at[here, :], ctxkv.at[here, :], cs, cr, dz * NY + y, tp)
 
-    for k in far_first:
+    for k in Z_ORDER:
         c_copy(k).start()
 
     phase("hidden_kv")
@@ -457,16 +451,8 @@
     mgsend[...] = total
     mgrecv[group] = total
 
-    def mg_copy(k):
-        g = lax.rem(group + k, NY * NTP)
-        dy, dt = lax.div(g, NTP), lax.rem(g, NTP)
-        return remote(mgsend, mgrecv.at[group], mgs, mgr, z * NY + dy, dt)
-
-    def mg_start(k, c):
-        mg_copy(k).start()
-        return c
-
-    lax.fori_loop(1, NY * NTP, mg_start, 0)
+    for k in G_ORDER:
+        remote(mgsend, mgrecv.at[group], mgs, mgr, *group_peer(k)).start()
 
     up_src = kvext.at[pl.ds(4 * TOK, TOK), :]
     dn_src = kvext.at[pl.ds(TOK, TOK), :]
@@ -508,6 +494,7 @@
     drain(qrecv.at[pl.ds(0, NY - 1)], qr)
     phase("c_wait")
     drain(ctxkv.at[pl.ds(0, CTX - NY * CTXL)], cr)
+    phase("attention")
     first = 1 - lax.div(x, 2)
     beside = x + 1 - 2 * lax.rem(x, 2)
     source = core * NY + y
@@ -517,31 +504,36 @@
             rsend.at[a, b, h], rrecv.at[a, source], rs, rr.at[a], z * NY + b, x * NC + h
         )
 
-    def pair(a, b):
-        p = 2 * b + a
-        xq = qrecv[b].astype(F32)
-        qp = jnp.where(low, jnp.where(a == 1, half_swap(xq), xq), 0.0).astype(BF16)
-        base = jnp.clip(row0 + 2 * p - 4, 0, LAST_START) - row0 + 4
-        rows = pl.ds(pl.multiple_of(base * GRID_W, GRID_W), 10 * GRID_W)
-        t = jnp.where(p < 2, p, jnp.where(p < 6, 2, p - 3))
-        sc_ctx = dot_nt(qp, ctxkv[...])
-        kvw = kvext[rows, :]
-        sc_win = dot_nt(qp, kvw) + btab[t]
+    def pairs(a, *blocks):
+        queries, windows = [], []
+        for b in blocks:
+            p = 2 * b + a
+            xq = qrecv[b].astype(F32)
+            queries.append(
+                jnp.where(low, jnp.where(a == 1, half_swap(xq), xq), 0.0).astype(BF16)
+            )
+            base = jnp.clip(row0 + 2 * p - 4, 0, LAST_START) - row0 + 4
+            rows = pl.ds(pl.multiple_of(base * GRID_W, GRID_W), 10 * GRID_W)
+            windows.append((rows, jnp.where(p < 2, p, jnp.where(p < 6, 2, p - 3))))
+        sc_ctx = dot_nt(jnp.concatenate(queries, axis=0), ctxkv[...])
+        sc_win = jnp.concatenate(
+            [dot_nt(qp, kvext[rows, :]) + btab[t] for qp, (rows, t) in zip(queries, windows)],
+            axis=0,
+        )
         top = jnp.maximum(
             jnp.max(sc_ctx, axis=1, keepdims=True), jnp.max(sc_win, axis=1, keepdims=True)
         )
         e_ctx = jnp.exp(sc_ctx - top)
         e_win = jnp.exp(sc_win - top)
         den = jnp.sum(e_ctx, axis=1, keepdims=True) + jnp.sum(e_win, axis=1, keepdims=True)
-        o = dot(e_ctx.astype(BF16), ctxkv[...]) + dot(e_win.astype(BF16), kvw)
-        o = o * (1.0 / den)
-        for h in range(NC):
-            r0, r1 = o[OUTR * h : OUTR * h + OUTR], o[64 + OUTR * h : 64 + OUTR * h + OUTR]
-            rsend[a, b, h] = jnp.where(low, half_swap(r0), r1).astype(BF16)
-
-    def pairs(a, *blocks):
-        for b in blocks:
-            pair(a, b)
+        e_win = e_win.astype(BF16)
+        o_all = dot(e_ctx.astype(BF16), ctxkv[...])
+        for i, (b, (rows, t)) in enumerate(zip(blocks, windows)):
+            part = slice(128 * i, 128 * i + 128)
+            o = (o_all[part] + dot(e_win[part], kvext[rows, :])) * (1.0 / den[part])
+            for h in range(NC):
+                r0, r1 = o[OUTR * h : OUTR * h + OUTR], o[64 + OUTR * h : 64 + OUTR * h + OUTR]
+                rsend[a, b, h] = jnp.where(low, half_swap(r0), r1).astype(BF16)
         for b in blocks:
             for h in range(NC):
                 here = (b == y) & (h == core)
@@ -590,8 +582,8 @@
     phase("attention2")
     pairs(first, 0, 3)
     phase("attention3")
+    pairs(1 - first, 0, 3)
     pairs(1 - first, 1, 2)
-    pairs(1 - first, 0, 3)
     phase("w_wait")
     w_copy.wait_recv()
     finish(first)

time: 45.7 us -> 45.2 us (0.989)
  Pallas kernels: 44.9 us -> 44.4 us
    pallas_call x1, Pallas kernels: 44.9 us -> 44.4 us  [shards(): pl.pallas_call(kernel, name='whole', out_shape=jax.ShapeDtypeStruct((OUTR...]
where the time goes in v5:
time: 45.2 us; the launch traced here: 45.1 us
  Pallas kernels  44.4 us (98%)
  local copies, waits for them, and re-layouts  0.66 us (1%)
    pallas_call x1, Pallas kernels, shards(): pl.pallas_call(kernel, name='whole', out_shape=jax.ShapeDtypeStruct((OUTR...  44.4 us

profile of v5, /device:TPU:1, one launch (start us, length us, event | category | flops | bytes accessed | tf_op | source)
XLA Modules:
  0.0 45.1 jit_solution(18358416226530165055)
XLA Ops:
  0.0 44.4 %whole.1 = bf16[32,2048]{1,0:T(8,128)(2,1)S(1)} custom-call(bf16[16,128]{1,0:T(8,128)(2,1)} %bitcast.8, bf16[16,128]{1,0:T(8,128)(2,1)} %bitcast.9, f32[16,128]{1,0:T(8,128)} %bitcast.6, f32[16,128]{1,0:T(8,128)} %bitcast.7, f32[15,4,31]{2,1,0:T(4,128)} %bitcast.5, bf16[256,2048]{1,0:T(8,128)(2,1)} %lat_h.1, bf16[32,2048]{1,0:T(8,128)(2,1)} %ctx_h.1, ...), custom_call_target="tpu_custom_call" | custom-call | tf_op jit(solution)/shard_map/whole/pallas_call | solution.py:678
  44.4 0.7 %copy.17 = bf16[32,2048]{1,0:T(8,128)(2,1)} copy(bf16[32,2048]{1,0:T(8,128)(2,1)S(1)} %whole.1) | data formatting | bytes 262144

commit v6 on v5

--- a/solution.py
+++ b/solution.py
@@ -20,7 +20,8 @@
 CTX = 1024
 OUTR = TOK // NTP
 LAST_START = NZ * NY * TOK // GRID_W - WIN_ROWS
-SPECIAL = (0, 1, 2, 6, 7)
+TABLES = 8
+WIN = WIN_ROWS * GRID_W
 Z_ORDER = (4, 3, 5, 2, 6, 1, 7)
 G_ORDER = sorted(
     ((ky, kx, kc) for ky in range(NY) for kx in range(NX) for kc in range(NC)),
@@ -128,6 +129,7 @@
     rrecv,
     gated,
     psend,
+    hop,
     precv,
     lsem,
     zs,
@@ -156,6 +158,7 @@
     rr,
     gs,
     gr,
+    hp,
     ps,
     pr,
 ):
@@ -291,32 +294,23 @@
 
     phase("tables")
     col = lax.rem(lax.broadcasted_iota(jnp.int32, (64, 128), 1), 64)
-    right = lax.div(lax.broadcasted_iota(jnp.int32, (64, 128), 1), 64)
     qcol = lax.broadcasted_iota(jnp.int32, (64, 128), 0)
     first_col = jnp.clip(qcol - WIN_COLS // 2, 0, GRID_W - WIN_COLS)
     in_cols = (col >= first_col) & (col < first_col + WIN_COLS)
     row0 = z * 16
 
     def table(t, c):
-        p = jnp.where(t < 3, t, t + 3)
-        base = jnp.clip(row0 + 2 * p - 4, 0, LAST_START)
-        for a in range(2):
-            row = row0 + 2 * p + a
-            off = jnp.clip(row - 4, 0, LAST_START) - base
-            d0 = base - row + 7
-            for m in range(5):
-                line = biasx[pl.ds(d0 + 2 * m, 1), :]
-                tile = pltpu.roll(
-                    jnp.broadcast_to(line, (64, 128)), 113, 1, stride=1, stride_axis=0
-                )
-                krow = right + 2 * m
-                ok = in_cols & (krow >= off) & (krow < off + WIN_ROWS)
-                btab[t, a * 64 : a * 64 + 64, m * 128 : m * 128 + 128] = jnp.where(
-                    ok, tile, -jnp.inf
-                )
+        row = row0 + jnp.where(t < 5, t, t + 8)
+        d0 = jnp.clip(row - 4, 0, LAST_START) - row + 7
+        for m in range(WIN_ROWS // 2):
+            line = biasx[pl.ds(d0 + 2 * m, 1), :]
+            tile = pltpu.roll(
+                jnp.broadcast_to(line, (64, 128)), 113, 1, stride=1, stride_axis=0
+            )
+            btab[t, :, m * 128 : m * 128 + 128] = jnp.where(in_cols, tile, -jnp.inf)
         return c
 
-    lax.fori_loop(0, len(SPECIAL), table, 0)
+    lax.fori_loop(0, TABLES, table, 0)
 
     @pl.when(z == 0)
     def _():
@@ -495,29 +489,28 @@
     phase("c_wait")
     drain(ctxkv.at[pl.ds(0, CTX - NY * CTXL)], cr)
     phase("attention")
-    first = 1 - lax.div(x, 2)
-    beside = x + 1 - 2 * lax.rem(x, 2)
+    across = lax.rem(x + 2, NX)
+    plus, minus = lax.rem(x + 1, NX), lax.rem(x + NX - 1, NX)
     source = core * NY + y
-
-    def r_copy(a, b, h):
+    fold = OUTR // 2
+
+    def r_copy(i, b, h):
         return remote(
-            rsend.at[a, b, h], rrecv.at[a, source], rs, rr.at[a], z * NY + b, x * NC + h
+            rsend.at[i, b, h], rrecv.at[i, source], rs, rr.at[i], z * NY + b, x * NC + h
         )
 
-    def pairs(a, *blocks):
+    def attend(i, *blocks):
         queries, windows = [], []
         for b in blocks:
-            p = 2 * b + a
-            xq = qrecv[b].astype(F32)
-            queries.append(
-                jnp.where(low, jnp.where(a == 1, half_swap(xq), xq), 0.0).astype(BF16)
-            )
-            base = jnp.clip(row0 + 2 * p - 4, 0, LAST_START) - row0 + 4
-            rows = pl.ds(pl.multiple_of(base * GRID_W, GRID_W), 10 * GRID_W)
-            windows.append((rows, jnp.where(p < 2, p, jnp.where(p < 6, 2, p - 3))))
+            xq = qrecv[b, pl.ds(pl.multiple_of(64 * lax.rem(i, 2), 64), 64), :].astype(F32)
+            queries.append(jnp.where(low, jnp.where(i > 1, half_swap(xq), xq), 0.0).astype(BF16))
+            row = 4 * b + i
+            base = jnp.clip(row0 + row - 4, 0, LAST_START) - row0 + 4
+            keys = pl.ds(pl.multiple_of(base * GRID_W, GRID_W), WIN)
+            windows.append((keys, jnp.where(row < 4, row, jnp.where(row < 13, 4, row - 8))))
         sc_ctx = dot_nt(jnp.concatenate(queries, axis=0), ctxkv[...])
         sc_win = jnp.concatenate(
-            [dot_nt(qp, kvext[rows, :]) + btab[t] for qp, (rows, t) in zip(queries, windows)],
+            [dot_nt(qp, kvext[keys, :]) + btab[t] for qp, (keys, t) in zip(queries, windows)],
             axis=0,
         )
         top = jnp.maximum(
@@ -528,47 +521,59 @@
         den = jnp.sum(e_ctx, axis=1, keepdims=True) + jnp.sum(e_win, axis=1, keepdims=True)
         e_win = e_win.astype(BF16)
         o_all = dot(e_ctx.astype(BF16), ctxkv[...])
-        for i, (b, (rows, t)) in enumerate(zip(blocks, windows)):
-            part = slice(128 * i, 128 * i + 128)
-            o = (o_all[part] + dot(e_win[part], kvext[rows, :])) * (1.0 / den[part])
+        for n, (b, (keys, t)) in enumerate(zip(blocks, windows)):
+            part = slice(64 * n, 64 * n + 64)
+            o = (o_all[part] + dot(e_win[part], kvext[keys, :])) * (1.0 / den[part])
             for h in range(NC):
-                r0, r1 = o[OUTR * h : OUTR * h + OUTR], o[64 + OUTR * h : 64 + OUTR * h + OUTR]
-                rsend[a, b, h] = jnp.where(low, half_swap(r0), r1).astype(BF16)
+                r0 = o[OUTR * h : OUTR * h + fold]
+                r1 = o[OUTR * h + fold : OUTR * h + OUTR]
+                rsend[i, b, h] = jnp.where(low, half_swap(r0), r1).astype(BF16)
         for b in blocks:
             for h in range(NC):
                 here = (b == y) & (h == core)
 
                 @pl.when(here)
                 def _():
-                    rrecv[a, source] = rsend[a, b, h]
+                    rrecv[i, source] = rsend[i, b, h]
 
                 @pl.when(jnp.logical_not(here))
                 def _():
-                    r_copy(a, b, h).start()
-
-    def p_copy(i):
-        return remote(psend.at[i], precv.at[x], ps, pr, sp, i * NC + core)
-
-    def finish(a):
-        phase("r_wait")
-        drain(rrecv.at[a, pl.ds(0, NC * NY - 1)], rr.at[a])
-        phase("project")
+                    r_copy(i, b, h).start()
+
+    def project(i, name, *steps):
+        phase("r_wait_" + name)
+        drain(rrecv.at[i, pl.ds(0, NC * NY - 1)], rr.at[i])
+        phase("project_" + name)
         for part in range(2):
             src = (core if part == 0 else 1 - core) * NY
             for q in range(2):
-                x0, x1 = rrecv[a, src + 2 * q].astype(F32), rrecv[a, src + 2 * q + 1].astype(F32)
+                x0, x1 = rrecv[i, src + 2 * q].astype(F32), rrecv[i, src + 2 * q + 1].astype(F32)
                 cols = slice(TOK * part + 128 * q, TOK * part + 128 * q + 128)
-                up = jnp.where(low, x0, half_swap(x1)) * sgate[2 * a, :, cols]
-                dn = jnp.where(low, half_swap(x0), x1) * sgate[2 * a + 1, :, cols]
-                gated[0:OUTR, cols] = up.astype(BF16)
-                gated[OUTR : 2 * OUTR, cols] = dn.astype(BF16)
-        for n in range(4):
-            cols = slice(512 * n, 512 * n + 512)
-            term = dot(gated[:, :TOK], wo[:, cols]) + dot(gated[:, TOK:], wo2[:, cols])
-            psend[2 * a, :, cols] = term[:OUTR].astype(BF16)
-            psend[2 * a + 1, :, cols] = term[OUTR:].astype(BF16)
-
-    pairs(first, 1, 2)
+                up = jnp.where(low, x0, half_swap(x1)) * sgate[i, 0:fold, cols]
+                dn = jnp.where(low, half_swap(x0), x1) * sgate[i, fold:OUTR, cols]
+                gated[0:fold, cols] = up.astype(BF16)
+                gated[fold:OUTR, cols] = dn.astype(BF16)
+        for pieces, then in steps:
+            for n in pieces:
+                cols = slice(512 * n, 512 * n + 512)
+                term = dot(gated[:, :TOK], wo[:, cols]) + dot(gated[:, TOK:], wo2[:, cols])
+                psend[i, :, cols] = term.astype(BF16)
+            then()
+
+    def to_neighbour(src, up, dst, sem):
+        remote(src, dst, ps, sem, sp, (plus if up else minus) * NC + core).start()
+
+    def send_across(*pieces):
+        for n in pieces:
+            src = psend.at[across, :, pl.ds(512 * n, 512)]
+            to_neighbour(src, n < 2, hop.at[n], hp.at[n])
+
+    def send_on(up, at, width):
+        cols = pl.ds(at, width)
+        src = psend.at[plus if up else minus, :, cols]
+        to_neighbour(src, up, precv.at[0 if up else 1, :, cols], pr)
+
+    attend(across, 1, 2)
     phase("h_wait")
 
     @pl.when(z > 0)
@@ -580,17 +585,31 @@
         dn_copy.wait_recv()
 
     phase("attention2")
-    pairs(first, 0, 3)
+    attend(across, 0, 3)
     phase("attention3")
-    pairs(1 - first, 0, 3)
-    pairs(1 - first, 1, 2)
-    phase("w_wait")
+    attend(plus, 0, 3, 1, 2)
+    phase("attention4")
+    attend(minus, 0, 3, 1, 2)
+    phase("attention5")
+    attend(x, 0, 3, 1, 2)
     w_copy.wait_recv()
-    finish(first)
-    p_copy(lax.rem(x + 2, NX)).start()
-    p_copy(lax.rem(beside + 2, NX)).start()
-    finish(1 - first)
-    p_copy(beside).start()
+    project(
+        across,
+        "across",
+        ((0, 2), lambda: send_across(0, 2)),
+        ((1, 3), lambda: send_across(1, 3)),
+    )
+    project(plus, "plus", ((2, 3, 0, 1), lambda: send_on(True, D // 2, D // 2)))
+    project(minus, "minus", ((0, 1, 2, 3), lambda: send_on(False, 0, D // 2)))
+    for n in (0, 2, 1, 3):
+        phase(f"hop{n}")
+        up, cols = n < 2, slice(512 * n, 512 * n + 512)
+        drain(hop.at[n], hp.at[n])
+        to = plus if up else minus
+        psend[to, :, cols] = (psend[to, :, cols].astype(F32) + hop[n].astype(F32)).astype(BF16)
+        send_on(up, 512 * n, 512)
+
+    project(x, "own", ((0, 1, 2, 3), lambda: None))
 
     phase("sent1")
     drain(zrecv.at[pl.ds(0, NZ - 1)], zs)
@@ -605,8 +624,8 @@
     drain(qrecv.at[pl.ds(0, NY - 1)], qs)
     w_copy.wait_send()
     g_copy.wait_send()
-    for a in range(2):
-        drain(rrecv.at[a, pl.ds(0, NC * NY - 1)], rs)
+    for i in range(NX):
+        drain(rrecv.at[i, pl.ds(0, NC * NY - 1)], rs)
 
     @pl.when(z < NZ - 1)
     def _():
@@ -621,18 +640,16 @@
         mod[4:5, 256 * t : 256 * t + 128] = total[0:1]
         mod[4:5, 256 * t + 128 : 256 * t + 256] = total[1:2]
     phase("p_wait")
-    drain(precv.at[pl.ds(0, NX - 1)], pr)
+    drain(precv, pr)
     phase("final")
-    branch = psend[x].astype(F32)
-    for k in (1, 2, 3):
-        branch = branch + precv[lax.rem(x + k, NX)].astype(F32)
+    branch = psend[x].astype(F32) + precv[0].astype(F32) + precv[1].astype(F32)
     branch = branch.astype(BF16).astype(F32)
     normed = branch * lax.rsqrt(jnp.mean(branch * branch, axis=1, keepdims=True) + EPSILON)
     own = lat[pl.ds(pl.multiple_of(tp * OUTR, OUTR), OUTR), :].astype(F32)
     out_ref[...] = (own + mod[4:5, :] * (normed * mod[6:7, :])).astype(BF16)
 
     phase("sent")
-    drain(precv.at[pl.ds(0, NX - 1)], ps)
+    drain(psend.at[pl.ds(0, NX - 1)], ps)
     phase(None)
 
 
@@ -705,7 +722,7 @@
             pltpu.VMEM((NY * NTP, 2, 128), F32),
             pltpu.VMEM((8, D), F32),
             pltpu.VMEM((4, 8, D), F32),
-            pltpu.VMEM((len(SPECIAL), 128, 640), F32),
+            pltpu.VMEM((TABLES, GRID_W, WIN), F32),
             pltpu.VMEM((TOK, D), BF16),
             pltpu.VMEM((NY * CTXL, D), BF16),
             pltpu.VMEM((TOK, 128), F32),
@@ -718,11 +735,12 @@
             pltpu.VMEM((NX, NC, OUTR, TOK), BF16),
             pltpu.VMEM((NX, OUTR, TOK), BF16),
             pltpu.VMEM((NX, OUTR, NC * TOK), F32),
-            pltpu.VMEM((2, NY, NC, OUTR, 128), BF16),
-            pltpu.VMEM((2, NC * NY, OUTR, 128), BF16),
-            pltpu.VMEM((2 * OUTR, NC * TOK), BF16),
+            pltpu.VMEM((NX, NY, NC, OUTR // 2, 128), BF16),
+            pltpu.VMEM((NX, NC * NY, OUTR // 2, 128), BF16),
+            pltpu.VMEM((OUTR, NC * TOK), BF16),
             pltpu.VMEM((NX, OUTR, D), BF16),
-            pltpu.VMEM((NX, OUTR, D), BF16),
+            pltpu.VMEM((4, OUTR, D // 4), BF16),
+            pltpu.VMEM((2, OUTR, D), BF16),
             dma((9,)),
             dma,
             dma,
@@ -747,9 +765,10 @@
             dma((2,)),
             dma((2,)),
             dma,
-            dma((2,)),
-            dma,
-            dma,
+            dma((NX,)),
+            dma,
+            dma,
+            dma((4,)),
             dma,
             dma,
         ],

time: 45.2 us -> 42.9 us (0.949)
  Pallas kernels: 44.4 us -> 42.1 us
    pallas_call x1, Pallas kernels: 44.4 us -> 42.1 us  [shards(): pl.pallas_call(kernel, name='whole', out_shape=jax.ShapeDtypeStruct((OUTR...]
where the time goes in v6:
time: 42.9 us; the launch traced here: 42.8 us
  Pallas kernels  42.1 us (98%)
  local copies, waits for them, and re-layouts  0.66 us (2%)
    pallas_call x1, Pallas kernels, shards(): pl.pallas_call(kernel, name='whole', out_shape=jax.ShapeDtypeStruct((OUTR...  42.1 us

profile of v6, /device:TPU:1, one launch (start us, length us, event | category | flops | bytes accessed | tf_op | source)
XLA Modules:
  0.0 42.8 jit_solution(4673699747447540857)
XLA Ops:
  0.0 42.1 %whole.1 = bf16[32,2048]{1,0:T(8,128)(2,1)S(1)} custom-call(bf16[16,128]{1,0:T(8,128)(2,1)} %bitcast.8, bf16[16,128]{1,0:T(8,128)(2,1)} %bitcast.9, f32[16,128]{1,0:T(8,128)} %bitcast.6, f32[16,128]{1,0:T(8,128)} %bitcast.7, f32[15,4,31]{2,1,0:T(4,128)} %bitcast.5, bf16[256,2048]{1,0:T(8,128)(2,1)} %lat_h.1, bf16[32,2048]{1,0:T(8,128)(2,1)} %ctx_h.1, ...), custom_call_target="tpu_custom_call" | custom-call | tf_op jit(solution)/shard_map/whole/pallas_call | solution.py:695
  42.2 0.7 %copy.17 = bf16[32,2048]{1,0:T(8,128)(2,1)} copy(bf16[32,2048]{1,0:T(8,128)(2,1)S(1)} %whole.1) | data formatting | bytes 262144

commit v7 on v6

--- a/solution.py
+++ b/solution.py
@@ -387,6 +387,13 @@
         c_copy(k).start()
 
     phase("hidden_kv")
+
+    def k_copy(k, i):
+        dy = lax.rem(y + k, NY)
+        at = pl.ds(pl.multiple_of((1 + y) * TOK + 128 * i, 128), 128)
+        src = kvsend.at[dy, pl.ds(128 * i, 128), :]
+        return remote(src, kvext.at[at, :], ks, kr.at[y], z * NY + dy, tp)
+
     for i in range(2):
         rows = slice(128 * i, 128 * i + 128)
         for n in range(4):
@@ -398,19 +405,14 @@
             vt = kv[:, 256 + 128 * q : 256 + 128 * q + 128]
             kvsend[2 * q, rows] = jnp.where(low, kt, half_swap(vt)).astype(BF16)
             kvsend[2 * q + 1, rows] = jnp.where(low, half_swap(kt), vt).astype(BF16)
-    mine = pl.ds(pl.multiple_of((1 + y) * TOK, TOK), TOK)
-    kvext[mine, :] = kvsend[y]
-
-    def k_copy(k):
-        dy = lax.rem(y + k, NY)
-        return remote(kvsend.at[dy], kvext.at[mine, :], ks, kr.at[y], z * NY + dy, tp)
+        for k in (2, 1, 3):
+            k_copy(k, i).start()
+        kvext[pl.ds(pl.multiple_of((1 + y) * TOK + 128 * i, 128), 128), :] = kvsend[y, rows]
 
     def k_in(dy):
         rows = pl.ds(pl.multiple_of((1 + dy) * TOK, TOK), TOK)
         return remote(kvsend.at[y], kvext.at[rows, :], ks, kr.at[dy], z * NY + dy, tp)
 
-    for k in (2, 1, 3):
-        k_copy(k).start()
 
     phase("qg")
     drain(wqg, lsem.at[7])
@@ -540,7 +542,7 @@
                 def _():
                     r_copy(i, b, h).start()
 
-    def project(i, name, *steps):
+    def gate(i, name, at):
         phase("r_wait_" + name)
         drain(rrecv.at[i, pl.ds(0, NC * NY - 1)], rr.at[i])
         phase("project_" + name)
@@ -551,14 +553,16 @@
                 cols = slice(TOK * part + 128 * q, TOK * part + 128 * q + 128)
                 up = jnp.where(low, x0, half_swap(x1)) * sgate[i, 0:fold, cols]
                 dn = jnp.where(low, half_swap(x0), x1) * sgate[i, fold:OUTR, cols]
-                gated[0:fold, cols] = up.astype(BF16)
-                gated[fold:OUTR, cols] = dn.astype(BF16)
-        for pieces, then in steps:
-            for n in pieces:
-                cols = slice(512 * n, 512 * n + 512)
-                term = dot(gated[:, :TOK], wo[:, cols]) + dot(gated[:, TOK:], wo2[:, cols])
-                psend[i, :, cols] = term.astype(BF16)
-            then()
+                gated[at : at + fold, cols] = up.astype(BF16)
+                gated[at + fold : at + OUTR, cols] = dn.astype(BF16)
+
+    def project(targets, at, *pieces):
+        rows = slice(at, at + OUTR * len(targets))
+        for n in pieces:
+            cols = slice(512 * n, 512 * n + 512)
+            term = dot(gated[rows, :TOK], wo[:, cols]) + dot(gated[rows, TOK:], wo2[:, cols])
+            for m, i in enumerate(targets):
+                psend[i, :, cols] = term[OUTR * m : OUTR * m + OUTR].astype(BF16)
 
     def to_neighbour(src, up, dst, sem):
         remote(src, dst, ps, sem, sp, (plus if up else minus) * NC + core).start()
@@ -593,15 +597,19 @@
     phase("attention5")
     attend(x, 0, 3, 1, 2)
     w_copy.wait_recv()
-    project(
-        across,
-        "across",
-        ((0, 2), lambda: send_across(0, 2)),
-        ((1, 3), lambda: send_across(1, 3)),
-    )
-    project(plus, "plus", ((2, 3, 0, 1), lambda: send_on(True, D // 2, D // 2)))
-    project(minus, "minus", ((0, 1, 2, 3), lambda: send_on(False, 0, D // 2)))
-    for n in (0, 2, 1, 3):
+    gate(across, "across", 0)
+    project((across,), 0, 0, 2)
+    send_across(0, 2)
+    project((across,), 0, 1, 3)
+    send_across(1, 3)
+    gate(plus, "plus", OUTR)
+    project((plus,), OUTR, 2, 3)
+    send_on(True, D // 2, D // 2)
+    gate(minus, "minus", 2 * OUTR)
+    project((plus, minus), OUTR, 0, 1)
+    send_on(False, 0, D // 2)
+
+    def add_and_send(n):
         phase(f"hop{n}")
         up, cols = n < 2, slice(512 * n, 512 * n + 512)
         drain(hop.at[n], hp.at[n])
@@ -609,7 +617,12 @@
         psend[to, :, cols] = (psend[to, :, cols].astype(F32) + hop[n].astype(F32)).astype(BF16)
         send_on(up, 512 * n, 512)
 
-    project(x, "own", ((0, 1, 2, 3), lambda: None))
+    phase("rest")
+    project((minus,), 2 * OUTR, 2, 3)
+    for n in (0, 2, 1, 3):
+        add_and_send(n)
+    gate(x, "own", 0)
+    project((x,), 0, 0, 1, 2, 3)
 
     phase("sent1")
     drain(zrecv.at[pl.ds(0, NZ - 1)], zs)
@@ -737,7 +750,7 @@
             pltpu.VMEM((NX, OUTR, NC * TOK), F32),
             pltpu.VMEM((NX, NY, NC, OUTR // 2, 128), BF16),
             pltpu.VMEM((NX, NC * NY, OUTR // 2, 128), BF16),
-            pltpu.VMEM((OUTR, NC * TOK), BF16),
+            pltpu.VMEM((3 * OUTR, NC * TOK), BF16),
             pltpu.VMEM((NX, OUTR, D), BF16),
             pltpu.VMEM((4, OUTR, D // 4), BF16),
             pltpu.VMEM((2, OUTR, D), BF16),

time: 42.9 us -> 42.6 us (level)
  no operation moved by 1% of the time
where the time goes in v7:
time: 42.6 us; the launch traced here: 42.5 us
  Pallas kernels  41.9 us (98%)
  local copies, waits for them, and re-layouts  0.66 us (2%)
    pallas_call x1, Pallas kernels, shards(): pl.pallas_call(kernel, name='whole', out_shape=jax.ShapeDtypeStruct((OUTR...  41.9 us

profile of v7, /device:TPU:1, one launch (start us, length us, event | category | flops | bytes accessed | tf_op | source)
XLA Modules:
  0.0 42.5 jit_solution(2662143743280006856)
XLA Ops:
  0.0 41.9 %whole.1 = bf16[32,2048]{1,0:T(8,128)(2,1)S(1)} custom-call(bf16[16,128]{1,0:T(8,128)(2,1)} %bitcast.8, bf16[16,128]{1,0:T(8,128)(2,1)} %bitcast.9, f32[16,128]{1,0:T(8,128)} %bitcast.6, f32[16,128]{1,0:T(8,128)} %bitcast.7, f32[15,4,31]{2,1,0:T(4,128)} %bitcast.5, bf16[256,2048]{1,0:T(8,128)(2,1)} %lat_h.1, bf16[32,2048]{1,0:T(8,128)(2,1)} %ctx_h.1, ...), custom_call_target="tpu_custom_call" | custom-call | tf_op jit(solution)/shard_map/whole/pallas_call | solution.py:708
  41.9 0.7 %copy.17 = bf16[32,2048]{1,0:T(8,128)(2,1)} copy(bf16[32,2048]{1,0:T(8,128)(2,1)S(1)} %whole.1) | data formatting | bytes 262144

commit v8 on v7

--- a/solution.py
+++ b/solution.py
@@ -457,19 +457,35 @@
     up_copy = remote(up_src, up_dst, hs.at[0], hr.at[0], jnp.minimum(z + 1, NZ - 1) * NY + y, tp)
     dn_copy = remote(dn_src, dn_dst, hs.at[1], hr.at[1], jnp.maximum(z - 1, 0) * NY + y, tp)
 
-    @pl.when(y != 3)
+    @pl.when((y == NY - 1) & (z < NZ - 1))
+    def _():
+        up_copy.start()
+
+    @pl.when((y == 0) & (z > 0))
+    def _():
+        dn_copy.start()
+
+    @pl.when(y == 1)
+    def _():
+        k_in(0).wait_recv()
+
+    @pl.when((y == 1) & (z > 0))
+    def _():
+        dn_copy.start()
+
+    @pl.when(y != NY - 1)
     def _():
         k_in(3).wait_recv()
 
-    @pl.when(z < NZ - 1)
+    @pl.when((y != NY - 1) & (z < NZ - 1))
     def _():
         up_copy.start()
 
-    @pl.when(y != 0)
+    @pl.when(y > 1)
     def _():
         k_in(0).wait_recv()
 
-    @pl.when(z > 0)
+    @pl.when((y > 1) & (z > 0))
     def _():
         dn_copy.start()
 
@@ -609,18 +625,20 @@
     project((plus, minus), OUTR, 0, 1)
     send_on(False, 0, D // 2)
 
-    def add_and_send(n):
-        phase(f"hop{n}")
-        up, cols = n < 2, slice(512 * n, 512 * n + 512)
+    def add_and_send(m, n):
+        phase(f"hop{m}")
+        cols = pl.ds(pl.multiple_of(512 * n, 512), 512)
         drain(hop.at[n], hp.at[n])
-        to = plus if up else minus
+        up = n < 2
+        to = jnp.where(up, plus, minus)
         psend[to, :, cols] = (psend[to, :, cols].astype(F32) + hop[n].astype(F32)).astype(BF16)
-        send_on(up, 512 * n, 512)
+        dst = precv.at[jnp.where(up, 0, 1), :, cols]
+        remote(psend.at[to, :, cols], dst, ps, pr, sp, to * NC + core).start()
 
     phase("rest")
     project((minus,), 2 * OUTR, 2, 3)
-    for n in (0, 2, 1, 3):
-        add_and_send(n)
+    for m, (inner, first, last) in enumerate(((0, 2, 0), (2, 3, 1), (1, 0, 2), (3, 1, 3))):
+        add_and_send(m, jnp.where(x == 0, first, jnp.where(x == NX - 1, last, inner)))
     gate(x, "own", 0)
     project((x,), 0, 0, 1, 2, 3)
 

time: 42.6 us -> 42.6 us (level)
  no operation moved by 1% of the time
where the time goes in v8:
time: 42.6 us; the launch traced here: 42.5 us
  Pallas kernels  41.9 us (98%)
  local copies, waits for them, and re-layouts  0.66 us (2%)
    pallas_call x1, Pallas kernels, shards(): pl.pallas_call(kernel, name='whole', out_shape=jax.ShapeDtypeStruct((OUTR...  41.9 us

profile of v8, /device:TPU:1, one launch (start us, length us, event | category | flops | bytes accessed | tf_op | source)
XLA Modules:
  0.0 42.5 jit_solution(6472775728426133933)
XLA Ops:
  0.0 41.9 %whole.1 = bf16[32,2048]{1,0:T(8,128)(2,1)S(1)} custom-call(bf16[16,128]{1,0:T(8,128)(2,1)} %bitcast.8, bf16[16,128]{1,0:T(8,128)(2,1)} %bitcast.9, f32[16,128]{1,0:T(8,128)} %bitcast.6, f32[16,128]{1,0:T(8,128)} %bitcast.7, f32[15,4,31]{2,1,0:T(4,128)} %bitcast.5, bf16[256,2048]{1,0:T(8,128)(2,1)} %lat_h.1, bf16[32,2048]{1,0:T(8,128)(2,1)} %ctx_h.1, ...), custom_call_target="tpu_custom_call" | custom-call | tf_op jit(solution)/shard_map/whole/pallas_call | solution.py:726
  41.9 0.7 %copy.17 = bf16[32,2048]{1,0:T(8,128)(2,1)} copy(bf16[32,2048]{1,0:T(8,128)(2,1)S(1)} %whole.1) | data formatting | bytes 262144

commit v9 on v8

--- a/solution.py
+++ b/solution.py
@@ -437,7 +437,6 @@
     g_copy.start()
     drain(wo, lsem.at[5])
     w_copy = remote(wo, wo2, ws, wr, sp, partner)
-    w_copy.start()
 
     phase("kq_wait")
     drain(zgrecv.at[pl.ds(0, NZ - 1)], zgr)
@@ -502,6 +501,7 @@
     for part in range(2):
         g = (gbuf[:, core] if part == 0 else gother[...]).astype(F32)
         sgate[:, :, TOK * part : TOK * part + TOK] = g * (1.0 / (1.0 + jnp.exp(-g)))
+    w_copy.start()
     phase("q_wait")
     drain(qrecv.at[pl.ds(0, NY - 1)], qr)
     phase("c_wait")

time: 42.6 us -> 42.6 us (level)
  no operation moved by 1% of the time
where the time goes in v9:
time: 42.6 us; the launch traced here: 42.5 us
  Pallas kernels  41.9 us (98%)
  local copies, waits for them, and re-layouts  0.66 us (2%)
    pallas_call x1, Pallas kernels, shards(): pl.pallas_call(kernel, name='whole', out_shape=jax.ShapeDtypeStruct((OUTR...  41.9 us

profile of v9, /device:TPU:1, one launch (start us, length us, event | category | flops | bytes accessed | tf_op | source)
XLA Modules:
  0.0 42.5 jit_solution(10580605185106806198)
XLA Ops:
  0.0 41.9 %whole.1 = bf16[32,2048]{1,0:T(8,128)(2,1)S(1)} custom-call(bf16[16,128]{1,0:T(8,128)(2,1)} %bitcast.8, bf16[16,128]{1,0:T(8,128)(2,1)} %bitcast.9, f32[16,128]{1,0:T(8,128)} %bitcast.6, f32[16,128]{1,0:T(8,128)} %bitcast.7, f32[15,4,31]{2,1,0:T(4,128)} %bitcast.5, bf16[256,2048]{1,0:T(8,128)(2,1)} %lat_h.1, bf16[32,2048]{1,0:T(8,128)(2,1)} %ctx_h.1, ...), custom_call_target="tpu_custom_call" | custom-call | tf_op jit(solution)/shard_map/whole/pallas_call | solution.py:726
  41.9 0.7 %copy.17 = bf16[32,2048]{1,0:T(8,128)(2,1)} copy(bf16[32,2048]{1,0:T(8,128)(2,1)S(1)} %whole.1) | data formatting | bytes 262144
